TPU v7x, 32 devices: a whole 2x2x4 slice. The times are simulated.
32 devices in a mesh: sp: 8 (over z, x), tp: 4 (over y, core).
Axes of the slice: x: 2, y: 2, z: 4, core: 2. Of those that a mesh axis runs over, the one named last changes fastest.
Arguments:
- receptance: bfloat16 [1024, 1024], P('sp', 'tp'), may hold values from -6 to 6
- key_by_head: bfloat16 [1024, 1024], P('sp', 'tp'), may hold values from -6 to 6
- value_head_rows: bfloat16 [1024, 1024], P('sp', 'tp'), may hold values from -6 to 6
- decay_preact: bfloat16 [1024, 1024], P('sp', 'tp'), may hold values from -13 to -0.5
- correction_preact: bfloat16 [1024, 1024], P('sp', 'tp'), may hold values from -7 to 3
- result_sigmoid_factor: bfloat16 [1024, 1024], P('sp', 'tp'), may hold values from -6 to 6
- key_rate_mixing: float32 [1024], P('tp'), may hold values from 0.3 to 0.9
- diagonal_current_factor: float32 [1024], P('tp'), may hold values from -0.6 to 0.6
- per_head_gain: float32 [1024], P('tp'), may hold values from 0.1 to 1.9
- per_head_bias: float32 [1024], P('tp'), may hold values from -1.5 to 1.5
- output_matrix: bfloat16 [1024, 2048], P('tp'), may hold values from -0.1875 to 0.1875
- residual: bfloat16 [1024, 2048], P('sp'), may hold values from -6 to 6
- expert_norm_gain: float32 [2048], replicated, may hold values from 0.1 to 1.9
- routes: int32 [1024, 8], P('sp'), may hold values from 0 to 31, all different within a row; in each aligned block of 128 rows (0 to 127, 128 to 255, ...) at most 48 rows name the same one
- chosen_expert_weight: float32 [1024, 8], P('sp'), may hold values from 0.05 to 0.6
- routed_gate_weight: bfloat16 [32, 2048, 512], P(('sp', 'tp')), may hold values from -0.125 to 0.125
- routed_up_weight: bfloat16 [32, 2048, 512], P(('sp', 'tp')), may hold values from -0.125 to 0.125
- routed_down_weight: bfloat16 [32, 512, 2048], P(('sp', 'tp')), may hold values from -0.25 to 0.25
- common_gate_weight: bfloat16 [2048, 512], P(None, 'tp'), may hold values from -0.125 to 0.125
- common_up_weight: bfloat16 [2048, 512], P(None, 'tp'), may hold values from -0.125 to 0.125
- common_down_weight: bfloat16 [512, 2048], P('tp'), may hold values from -0.25 to 0.25
Outputs:
- layer_out: bfloat16 [1024, 2048], P('sp', 'tp')
Inputs may be any that keep to these rules, and one draw needn't show every extreme that they name: `routes`: each row names 8 different experts; in each aligned block of 128 rows no expert is named by more than 48 rows.
All inputs are finite; a program needn't handle non-finite values.
Results may differ from a plain program's by a relative error of at most 0.018.
Values may be sent and summed in bfloat16 or wider, within the bound.
A program may use at most 64 MiB of HBM per device.

v0:
```python
import jax
import jax.numpy as jnp
from jax import lax
from jax.sharding import PartitionSpec as P

CHANNEL_SPAN = 64


NORM_EPS = 1e-06
GROUP_EPS = 0.00064
HIGHEST = lax.Precision.HIGHEST


def entering_2(array, axis, combine, identity):
    peers, position = (lax.axis_size(axis), lax.axis_index(axis))
    everything = jax.tree.map(lambda part: lax.all_gather(part, axis), array)
    start = jax.tree.map(
        lambda part, zero: jnp.broadcast_to(jnp.asarray(zero, part.dtype), part.shape),
        array,
        identity,
    )

    def hop(k, before):
        reached = k < position
        new = combine(before, jax.tree.map(lambda part: part[k], everything))
        return jax.tree.map(lambda a, b: jnp.where(reached, a, b), new, before)

    return lax.fori_loop(0, peers, hop, start)


def partition_channels(source, head_size):
    row_count, col_count = source.shape
    return source.astype(jnp.float32).reshape(row_count, col_count // head_size, head_size)


def prepare(
    receptance, key_by_head, value_head_rows, decay_preact, correction_preact, key_rate_mixing
):
    key_rows = partition_channels(key_by_head, CHANNEL_SPAN)
    learning = jax.nn.sigmoid(partition_channels(correction_preact, CHANNEL_SPAN))
    length = jnp.sqrt(jnp.sum(key_rows * key_rows, axis=-1, keepdims=True))
    unit_keys = key_rows / jnp.maximum(length, 1.0)
    mix_rows = key_rate_mixing.reshape(1, key_rows.shape[1], CHANNEL_SPAN)
    interpolated_lookup_vectors = key_rows * (1.0 + (learning - 1.0) * mix_rows)
    log_decay = -jnp.exp(-jax.nn.softplus(-partition_channels(decay_preact, CHANNEL_SPAN)) - 0.5)
    return (
        partition_channels(receptance, CHANNEL_SPAN),
        interpolated_lookup_vectors,
        partition_channels(value_head_rows, CHANNEL_SPAN),
        log_decay,
        unit_keys,
        learning,
    )


def finalize(
    state_readout,
    query_vectors_partitioned,
    interpolated_lookup_vectors,
    content_vectors_partitioned,
    per_head_gain,
    per_head_bias,
    diagonal_current_factor,
    result_sigmoid_factor,
):
    shard_attention_count = state_readout.shape[1]
    average = jnp.mean(state_readout, axis=-1, keepdims=True)
    centred = state_readout - average
    variance = jnp.mean(centred * centred, axis=-1, keepdims=True)
    standardized_channels = centred * lax.rsqrt(variance + GROUP_EPS)
    standardized_channels = standardized_channels * per_head_gain.reshape(
        1, shard_attention_count, CHANNEL_SPAN
    ) + per_head_bias.reshape(1, shard_attention_count, CHANNEL_SPAN)
    diagonal_extra_contribution = (
        jnp.sum(
            query_vectors_partitioned
            * interpolated_lookup_vectors
            * diagonal_current_factor.reshape(1, shard_attention_count, CHANNEL_SPAN),
            axis=-1,
            keepdims=True,
        )
        * content_vectors_partitioned
    )
    concatenated_channels = (
        standardized_channels + diagonal_extra_contribution
    ) * partition_channels(result_sigmoid_factor, CHANNEL_SPAN)
    return concatenated_channels.reshape(
        state_readout.shape[0], shard_attention_count * CHANNEL_SPAN
    ).astype(jnp.bfloat16)


def expert_apply(rows_in, gate_weight, up_weight, down_weight):
    gate_part = jnp.dot(rows_in, gate_weight, preferred_element_type=jnp.float32)
    up_part = jnp.dot(rows_in, up_weight, preferred_element_type=jnp.float32)
    hidden = (jax.nn.silu(gate_part) * up_part).astype(jnp.bfloat16)
    return jnp.dot(hidden, down_weight, preferred_element_type=jnp.float32)


def to_blocks(source, span_len):
    row_count, head_count, head_size = source.shape
    return source.reshape(row_count // span_len, span_len, head_count, head_size).transpose(
        0, 2, 1, 3
    )


def from_blocks(source):
    block_count, head_count, span_len, head_size = source.shape
    return source.transpose(0, 2, 1, 3).reshape(block_count * span_len, head_count, head_size)


def compose(former, latter):
    return (
        jnp.matmul(former[0], latter[0], precision=HIGHEST),
        jnp.matmul(former[1], latter[0], precision=HIGHEST) + latter[1],
    )


def pair_products(left_rows, right_rows, keep_mask):
    return jnp.where(
        keep_mask, jnp.einsum("bhtn,bhsn->bhts", left_rows, right_rows, precision=HIGHEST), 0.0
    )


def unit_lower_inverse(strict_part, span_len):
    inverse = jnp.eye(span_len, dtype=jnp.float32) + strict_part
    power = strict_part
    covered = 1
    while covered < span_len - 1:
        power = jnp.matmul(power, power, precision=HIGHEST)
        inverse = inverse + jnp.matmul(inverse, power, precision=HIGHEST)
        covered = 2 * covered + 1
    return inverse


def block_terms(recept, interpolated_lookup_vectors, values, log_decay, unit_keys, learning):
    span_len = recept.shape[2]
    head_size = recept.shape[3]
    cumulative = jnp.cumsum(log_decay, axis=2)
    before = -jnp.exp(cumulative - log_decay) * unit_keys
    inverse_decay = jnp.exp(-cumulative)
    erase_cols = inverse_decay * unit_keys * learning
    write_cols = inverse_decay * interpolated_lookup_vectors
    read_rows = jnp.exp(cumulative) * recept
    later_row = lax.broadcasted_iota(jnp.int32, (span_len, span_len), 0)
    earlier_col = lax.broadcasted_iota(jnp.int32, (span_len, span_len), 1)
    strict = later_row > earlier_col
    inclusive = later_row >= earlier_col
    erase_pairs = pair_products(before, erase_cols, strict)
    write_pairs = pair_products(before, write_cols, strict)
    read_erase = pair_products(read_rows, erase_cols, inclusive)
    read_write = pair_products(read_rows, write_cols, inclusive)
    system_inverse = unit_lower_inverse(erase_pairs, span_len)
    right_side = jnp.concatenate(
        [jnp.einsum("bhts,bhsn->bhtn", write_pairs, values, precision=HIGHEST), before], axis=-1
    )
    solved = jnp.matmul(system_inverse, right_side, precision=HIGHEST)
    removed = solved[..., :head_size]
    carried = solved[..., head_size:]
    local_out = jnp.einsum("bhts,bhsn->bhtn", read_erase, removed, precision=HIGHEST) + jnp.einsum(
        "bhts,bhsn->bhtn", read_write, values, precision=HIGHEST
    )
    query_eff = read_rows + jnp.einsum("bhts,bhsn->bhtn", read_erase, carried, precision=HIGHEST)
    final_decay = jnp.exp(cumulative[:, :, span_len - 1 :, :])
    erase_end = final_decay * erase_cols
    write_end = final_decay * write_cols
    transit = (
        jnp.einsum("bhtj,bhtk->bhjk", carried, erase_end, precision=HIGHEST)
        + jnp.eye(head_size, dtype=jnp.float32) * final_decay
    )
    contrib = jnp.einsum("bhti,bhtk->bhik", removed, erase_end, precision=HIGHEST) + jnp.einsum(
        "bhti,bhtk->bhik", values, write_end, precision=HIGHEST
    )
    return (local_out, query_eff, transit, contrib)


def memory_heads(
    query_vectors_partitioned,
    interpolated_lookup_vectors,
    content_vectors_partitioned,
    log_decay,
    unit_keys,
    learning,
):
    span_len = min(64, query_vectors_partitioned.shape[0])
    local_out, query_eff, transit, contrib = block_terms(
        to_blocks(query_vectors_partitioned, span_len),
        to_blocks(interpolated_lookup_vectors, span_len),
        to_blocks(content_vectors_partitioned, span_len),
        to_blocks(log_decay, span_len),
        to_blocks(unit_keys, span_len),
        to_blocks(learning, span_len),
    )
    inner_p, inner_c = lax.associative_scan(compose, (transit, contrib), axis=0)
    totals = (inner_p[-1], inner_c[-1])
    head_count = transit.shape[1]
    head_size = transit.shape[2]
    identity_p = jnp.broadcast_to(
        jnp.eye(head_size, dtype=jnp.float32), (head_count, head_size, head_size)
    )
    zero_maps = jnp.zeros_like(identity_p)
    prefix = entering_2(totals, "sp", compose, (identity_p, zero_maps))
    entering = prefix[1]
    start_p = jnp.concatenate([identity_p[None], inner_p[:-1]], axis=0)
    start_c = jnp.concatenate([zero_maps[None], inner_c[:-1]], axis=0)
    state_in = jnp.matmul(entering[None], start_p, precision=HIGHEST) + start_c
    state_readout = local_out + jnp.einsum(
        "bhtj,bhij->bhti", query_eff, state_in, precision=HIGHEST
    )
    return from_blocks(state_readout)


def per_device(
    receptance,
    key_by_head,
    value_head_rows,
    decay_preact,
    correction_preact,
    result_sigmoid_factor,
    key_rate_mixing,
    diagonal_current_factor,
    per_head_gain,
    per_head_bias,
    output_matrix,
    residual,
    expert_norm_gain,
    routes,
    chosen_expert_weight,
    routed_gate_weight,
    routed_up_weight,
    routed_down_weight,
    common_gate_weight,
    common_up_weight,
    common_down_weight,
):
    (
        query_vectors_partitioned,
        interpolated_lookup_vectors,
        content_vectors_partitioned,
        log_decay,
        unit_keys,
        learning,
    ) = prepare(
        receptance, key_by_head, value_head_rows, decay_preact, correction_preact, key_rate_mixing
    )
    state_readout = memory_heads(
        query_vectors_partitioned,
        interpolated_lookup_vectors,
        content_vectors_partitioned,
        log_decay,
        unit_keys,
        learning,
    )
    blended_heads = finalize(
        state_readout,
        query_vectors_partitioned,
        interpolated_lookup_vectors,
        content_vectors_partitioned,
        per_head_gain,
        per_head_bias,
        diagonal_current_factor,
        result_sigmoid_factor,
    )
    whole_heads = lax.all_gather(blended_heads, "tp", axis=1, tiled=True)
    projected = jnp.dot(
        whole_heads,
        lax.all_gather(output_matrix, "tp", axis=0, tiled=True),
        preferred_element_type=jnp.float32,
    )
    middle = (residual.astype(jnp.float32) + projected).astype(jnp.bfloat16)
    middle_full = middle.astype(jnp.float32)
    row_scale = lax.rsqrt(jnp.mean(middle_full * middle_full, axis=-1, keepdims=True) + NORM_EPS)
    normed = (middle_full * row_scale * expert_norm_gain).astype(jnp.bfloat16)
    tp_index = lax.axis_index("tp")
    tp_count = lax.axis_size("tp")
    sp_count = lax.axis_size("sp")
    token_count, top_count = routes.shape
    model_width = normed.shape[1]
    capacity = 3 * token_count * top_count // (2 * sp_count * tp_count)
    owned_routes = routes % tp_count == tp_index
    target = routes // tp_count
    places = jnp.arange(sp_count, dtype=jnp.int32)
    hit_counts = jnp.sum(
        jnp.where(owned_routes[:, :, None] & (target[:, :, None] == places[None, None, :]), 1, 0),
        axis=1,
    ).astype(jnp.int32)
    earlier = jnp.cumsum(hit_counts, axis=0) - hit_counts
    within = jnp.take_along_axis(earlier, target, axis=1)
    slot_index = target * capacity + within
    dropped = sp_count * capacity
    flat_slots = jnp.where(owned_routes, slot_index, dropped).reshape(-1)
    token_ids = jnp.broadcast_to(jnp.arange(token_count, dtype=jnp.int32)[:, None], routes.shape)
    slot_tokens = (
        jnp.full((dropped,), token_count, jnp.int32)
        .at[flat_slots]
        .set(token_ids.reshape(-1), mode="drop")
    )
    slot_weights = (
        jnp.zeros((dropped,), jnp.float32)
        .at[flat_slots]
        .set(chosen_expert_weight.reshape(-1), mode="drop")
    )
    padded = jnp.concatenate([normed, jnp.zeros((1, model_width), jnp.bfloat16)], axis=0)
    outgoing = padded[slot_tokens].reshape(sp_count, capacity, model_width)
    arrived = lax.all_to_all(outgoing, "sp", split_axis=0, concat_axis=0, tiled=True)
    source_count, item_count, feature_count = arrived.shape
    flat_rows = arrived.reshape(source_count * item_count, feature_count)
    answer = expert_apply(
        flat_rows, routed_gate_weight[0], routed_up_weight[0], routed_down_weight[0]
    ).astype(jnp.bfloat16)
    returned = lax.all_to_all(
        answer.reshape(source_count, item_count, feature_count),
        "sp",
        split_axis=0,
        concat_axis=0,
        tiled=True,
    )
    flat_back = returned.reshape(dropped, model_width)
    token_rows = jnp.arange(token_count, dtype=jnp.int32)
    combine_table = jnp.where(
        slot_tokens[None, :] == token_rows[:, None], slot_weights[None, :], 0.0
    )
    routed = jnp.dot(combine_table, flat_back.astype(jnp.float32), precision=HIGHEST)
    shared_out = expert_apply(normed, common_gate_weight, common_up_weight, common_down_weight)
    summed = lax.psum_scatter(
        (routed + shared_out).astype(jnp.bfloat16), "tp", scatter_dimension=1, tiled=True
    ).astype(jnp.float32)
    col_count = summed.shape[1]
    own_cols = lax.dynamic_slice_in_dim(middle, tp_index * col_count, col_count, 1)
    return (own_cols.astype(jnp.float32) + summed).astype(jnp.bfloat16)


def solution(mesh):
    return jax.shard_map(
        per_device,
        mesh=mesh,
        in_specs=(
            P("sp", "tp"),
            P("sp", "tp"),
            P("sp", "tp"),
            P("sp", "tp"),
            P("sp", "tp"),
            P("sp", "tp"),
            P("tp"),
            P("tp"),
            P("tp"),
            P("tp"),
            P("tp", None),
            P("sp", None),
            P(),
            P("sp", None),
            P("sp", None),
            P(("sp", "tp"), None, None),
            P(("sp", "tp"), None, None),
            P(("sp", "tp"), None, None),
            P(None, "tp"),
            P(None, "tp"),
            P("tp", None),
        ),
        out_specs=P("sp", "tp"),
        check_vma=False,
    )
```

profile of v0, /device:TPU:0, one launch (start us, length us, event | category | flops | bytes accessed | tf_op | source)
XLA Modules:
  0.0 289.0 jit_solution(4621380416738040855)
XLA Ops:
  12.9 1.4 bitcast_multiply_fusion
  21.3 1.5 convolution_add_fusion.2
  28.4 1.6 copy.116
  31.0 1.5 convert_element_type.70
  32.5 1.6 fusion.64
  34.2 36.6 %all_gather.13 = f32[8,4,64,64]{3,2,1,0:T(8,128)} all-gather(f32[1,4,64,64]{3,2,1,0:T(8,128)S(1)} %get-tuple-element.153), channel_id=1, replica_groups=mesh['sp'=8,'tp'=4] {'sp'}, dimensions={0}, use_global_device_ids=true | all-gather | bytes 589824 | tf_op jit(solution)/shard_map/all_gather | solution.py:16
  70.8 1.6 fusion.63
  72.4 35.1 %all_gather.12 = f32[8,4,64,64]{3,2,1,0:T(8,128)} all-gather(f32[1,4,64,64]{3,2,1,0:T(8,128)S(1)} %get-tuple-element.155), channel_id=1, replica_groups=mesh['sp'=8,'tp'=4] {'sp'}, dimensions={0}, use_global_device_ids=true | all-gather | bytes 589824 | tf_op jit(solution)/shard_map/all_gather | solution.py:16
  108.4 19.0 %while.14 = (s32[]{:T(128)}, f32[4,64,64]{1,2,0:T(8,128)S(1)}, s32[]{:T(128)}, f32[8,4,64,64]{3,2,1,0:T(8,128)}, f32[8,4,64,64]{3,2,1,0:T(8,128)}, /*index=5*/s32[]{:T(128)}, s32[]{:T(128)}) while((s32[]{:T(128)}, f32[4,64,64]{1,2,0:T(8,128)S(1)}, s32[]{:T(128)}, f32[8,4,64,64]{3,2,1,0:T(8,128)}, f32[8,4,64,64]{3,2,1,0:T(8,128)}, ...), condition=%wide.region_3.4_spmd.clone, body=%wide.region_2.3_spmd.clone.sunk | while | flops 12648452 | bytes 985187 | solution.py:28
  109.4 1.3 fusion.161
  111.8 1.3 fusion.161
  114.2 1.3 fusion.161
  116.5 1.3 fusion.161
  118.9 1.3 fusion.161
  126.1 1.3 fusion.161
  128.2 1.4 fusion.24
  129.6 1.5 convolution_select_fusion.3
  136.1 7.1 %gather_fusion.1 = s32[1024]{0:T(1024)S(1)} fusion(s32[128,8]{1,0:T(8,128)S(1)} %sub.47, s32[1024]{0:T(1024)S(1)} %reshape.197), kind=kCustom, calls=%fused_computation.1 | custom fusion | bytes 16384 | tf_op jit(solution)/shard_map/jit(take_along_axis)/gather | solution.py:287
  143.6 4.3 %scatter_custom_fusion = s32[384]{0:T(512)S(1)} fusion(s32[1024]{0:T(1024)S(1)} %bitcast.181, s32[1024]{0:T(1024)S(1)} %reshape.207, s32[]{:T(128)} %constant.114.clone.1), kind=kCustom, calls=%fused_computation.166 | custom fusion | bytes 1540 | tf_op jit(solution)/shard_map/scatter | solution.py:295
  148.8 5.8 %all_gather.14 = bf16[128,1024]{1,0:T(8,128)(2,1)S(1)} all-gather(bf16[128,256]{1,0:T(8,128)(2,1)S(1)} %multiply_convert_fusion), channel_id=1, replica_groups=mesh['sp'=8,'tp'=4] {'tp'}, dimensions={1}, use_global_device_ids=true | all-gather | bytes 327680 | tf_op jit(solution)/shard_map/all_gather | solution.py:263
  154.6 3.1 %fusion.28 = (f32[128]{0:T(128)S(1)}, bf16[128,2048]{1,0:T(8,128)(2,1)S(1)}) fusion(bf16[128,1024]{1,0:T(8,128)(2,1)S(1)} %all_gather.14, bf16[1024,2048]{1,0:T(8,128)(2,1)} %all-gather.2.cloned.1.call-done, bf16[128,2048]{1,0:T(8,128)(2,1)S(1)} %copy-done.13), kind=kOutput, calls=%fused_computation.53 | convolution fusion | flops 538443648 | bytes 5505536 | tf_op jit(solution)/shard_map/dot_general | solution.py:264
  158.8 3.1 %gather_fusion = bf16[384,2048]{1,0:T(8,128)(2,1)} fusion(bf16[129,2048]{1,0:T(8,128)(2,1)S(1)} %concatenate.15, s32[1024]{0:T(1024)S(1)} %pad_clamp_fusion), kind=kCustom, calls=%fused_computation | custom fusion | bytes 3147264 | tf_op jit(solution)/shard_map/gather | solution.py:303
  161.9 43.2 %all_to_all.10 = bf16[8,48,2048]{2,1,0:T(8,128)(2,1)S(1)} all-to-all(bf16[8,48,2048]{2,1,0:T(8,128)(2,1)} %bitcast.169), channel_id=1, replica_groups=mesh['sp'=8,'tp'=4] {'sp'}, dimensions={0} | all-to-all | bytes 3145728 | tf_op jit(solution)/shard_map/all_to_all | solution.py:304
  207.3 5.1 %convolution_convert_fusion = bf16[384,2048]{1,0:T(8,128)(2,1)} fusion(bf16[1,512,2048]{2,1,0:T(8,128)(2,1)S(1)} %copy-done, bf16[384,2048]{1,0:T(8,128)(2,1)} %bitcast.172, bf16[1,2048,512]{2,1,0:T(8,128)(2,1)} %param.39, f32[384,512]{1,0:T(8,128)S(1)} %fusion.15), kind=kOutput, calls=%fused_computation.16 | convolution fusion | flops 1612578816 | bytes 8126464 | tf_op jit(solution)/shard_map/dot_general | solution.py:96
  212.4 4.4 %all-to-all-start.1 = ((bf16[8,48,2048]{2,1,0:T(8,128)(2,1)}), bf16[8,48,2048]{2,1,0:T(8,128)(2,1)}, u32[]{:S(2)}, u32[]{:S(2)}) async-start(bf16[8,48,2048]{2,1,0:T(8,128)(2,1)} %bitcast.170), calls=%async_computation.1 | async-start | bytes 3145728 | tf_op jit(solution)/shard_map/all_to_all | solution.py:310
  217.3 4.3 %scatter_custom_fusion.1 = f32[384]{0:T(512)S(1)} fusion(s32[1024]{0:T(1024)S(1)} %bitcast.182, f32[1024]{0:T(1024)S(1)} %reshape.215, f32[]{:T(128)} %constant.102.clone.1), kind=kCustom, calls=%fused_computation.164 | custom fusion | bytes 1540 | tf_op jit(solution)/shard_map/scatter | solution.py:300
  221.6 1.3 fusion.113
  223.0 30.5 %all-to-all-done.1 = bf16[8,48,2048]{2,1,0:T(8,128)(2,1)} async-done(((bf16[8,48,2048]{2,1,0:T(8,128)(2,1)}), bf16[8,48,2048]{2,1,0:T(8,128)(2,1)}, u32[]{:S(2)}, u32[]{:S(2)}) %all-to-all-start.1) | async-done | bytes 1572896 | tf_op jit(solution)/shard_map/all_to_all | solution.py:310
  253.5 3.4 %fusion.61 = f32[128,2048]{1,0:T(8,128)} fusion(bf16[384,2048]{1,0:T(8,128)(2,1)} %bitcast.32, f32[384]{0:T(512)S(1)} %scatter_custom_fusion.1, s32[384]{0:T(512)S(1)} %scatter_custom_fusion), kind=kOutput, calls=%fused_computation.97 | convolution fusion | flops 1208057856 | bytes 2624512 | tf_op jit(solution)/shard_map/dot_general | solution.py:322
  256.8 2.7 fusion.11
  259.6 20.9 %reduce-scatter.2.cloned.1.call-done = bf16[128,512]{1,0:T(8,128)(2,1)} async-done(((bf16[128,2048]{1,0:T(8,128)(2,1)}), bf16[128,512]{1,0:T(8,128)(2,1)}) %reduce-scatter.2.cloned.1.call-update) | async-done | bytes 131088 | tf_op jit(solution)/shard_map/reduce_scatter | solution.py:324
  280.5 1.7 add_convert_fusion
  (170 shorter events, 41.8 us)
Async XLA Ops:
  6.5 200.7 %copy-start = (bf16[1,512,2048]{2,1,0:T(8,128)(2,1)S(1)}, bf16[1,512,2048]{2,1,0:T(8,128)(2,1)}, u32[]{:S(2)}) copy-start(bf16[1,512,2048]{2,1,0:T(8,128)(2,1)} %param.40) | copy-start | bytes 6291460
  6.5 4.1 %copy-start.15 = (bf16[128,256]{1,0:T(8,128)(2,1)S(1)}, bf16[128,256]{1,0:T(8,128)(2,1)}, u32[]{:S(2)}) copy-start(bf16[128,256]{1,0:T(8,128)(2,1)} %param.27) | copy-start | bytes 196612
  6.5 6.0 %copy-start.21 = (f32[256]{0:T(256)S(1)}, f32[256]{0:T(256)}, u32[]{:S(2)}) copy-start(f32[256]{0:T(256)} %param.29) | copy-start | bytes 3076
  6.5 148.1 %all-gather.2.cloned.1.call-start = ((), (), s32[]{:S(2)}) async-start(), calls=%async_computation.3 | async-start | bytes 5242880 | tf_op jit(solution)/shard_map/all_gather | solution.py:266
  8.2 4.3 %copy-start.6 = (bf16[128,256]{0,1:T(8,128)(2,1)}, bf16[128,256]{0,1:T(8,128)(2,1)S(1)}, u32[]{:S(2)}) copy-start(bf16[128,256]{0,1:T(8,128)(2,1)S(1)} %copy.119) | copy-start | bytes 196612
  8.5 7.1 %copy-start.9 = (f32[64,64]{1,0:T(8,128)}, f32[64,64]{1,0:T(8,128)S(1)}, u32[]{:S(2)}) copy-start(f32[64,64]{1,0:T(8,128)S(1)} %fusion.93) | copy-start | bytes 49156
  21.3 3.9 %copy-start.3 = (bf16[2,64,4,64]{3,2,1,0:T(4,128)(2,1)}, bf16[2,64,4,64]{3,2,1,0:T(4,128)(2,1)S(1)}, u32[]{:S(2)}) copy-start(bf16[2,64,4,64]{3,2,1,0:T(4,128)(2,1)S(1)} %reshape_reshape.7) | copy-start | bytes 196612
  21.3 2.9 copy-start.10
  127.4 4.4 %copy-start.1 = (f32[2,64,4,64]{3,1,2,0:T(8,128)S(1)}, f32[2,64,4,64]{3,1,2,0:T(8,128)}, u32[]{:S(2)}) copy-start(f32[2,64,4,64]{3,1,2,0:T(8,128)} %copy.118) | copy-start | bytes 393220
  127.4 4.9 %copy-start.4 = (bf16[2,64,4,64]{3,2,1,0:T(4,128)(2,1)S(1)}, bf16[2,64,4,64]{3,2,1,0:T(4,128)(2,1)}, u32[]{:S(2)}) copy-start(bf16[2,64,4,64]{3,2,1,0:T(4,128)(2,1)} %copy-done.3) | copy-start | bytes 196612
  132.7 2.0 copy-start.22
  132.7 2.0 copy-start.7
  132.7 2.0 copy-start.11
  132.8 2.0 copy-start.12
  133.2 2.1 copy-start.17
  136.1 11.8 %copy-start.14 = (bf16[128,256]{1,0:T(8,128)(2,1)S(1)}, bf16[128,256]{1,0:T(8,128)(2,1)}, u32[]{:S(2)}) copy-start(bf16[128,256]{1,0:T(8,128)(2,1)} %param.25) | copy-start | bytes 196612
  136.1 11.8 %copy-start.19 = (f32[256]{0:T(256)S(1)}, f32[256]{0:T(256)}, u32[]{:S(2)}) copy-start(f32[256]{0:T(256)} %param.32) | copy-start | bytes 3076
  136.1 11.8 %copy-start.20 = (f32[256]{0:T(256)S(1)}, f32[256]{0:T(256)}, u32[]{:S(2)}) copy-start(f32[256]{0:T(256)} %param.31) | copy-start | bytes 3076
  136.1 18.5 %copy-start.13 = (bf16[128,2048]{1,0:T(8,128)(2,1)S(1)}, bf16[128,2048]{1,0:T(8,128)(2,1)}, u32[]{:S(2)}) copy-start(bf16[128,2048]{1,0:T(8,128)(2,1)} %param.34) | copy-start | bytes 1572868
  154.6 3.9 %copy-start.16 = (f32[2048]{0:T(1024)S(1)}, f32[2048]{0:T(1024)}, u32[]{:S(2)}) copy-start(f32[2048]{0:T(1024)} %param.35) | copy-start | bytes 24580
  157.7 0.8 copy-start.2
  161.9 44.4 %copy-start.23 = (bf16[1,2048,512]{2,1,0:T(8,128)(2,1)S(1)}, bf16[1,2048,512]{2,1,0:T(8,128)(2,1)}, u32[]{:S(2)}) copy-start(bf16[1,2048,512]{2,1,0:T(8,128)(2,1)} %param.38) | copy-start | bytes 6291460
  205.1 1.1 copy-start.5
  212.4 4.7 %copy-start.18 = (f32[128,8]{0,1:T(8,128)S(1)}, f32[128,8]{0,1:T(8,128)}, u32[]{:S(2)}) copy-start(f32[128,8]{0,1:T(8,128)} %param.37) | copy-start | bytes 12292
  212.4 41.1 %all-to-all-start.1 = ((bf16[8,48,2048]{2,1,0:T(8,128)(2,1)}), bf16[8,48,2048]{2,1,0:T(8,128)(2,1)}, u32[]{:S(2)}, u32[]{:S(2)}) async-start(bf16[8,48,2048]{2,1,0:T(8,128)(2,1)} %bitcast.170), calls=%async_computation.1 | async-start | bytes 3145728 | tf_op jit(solution)/shard_map/all_to_all | solution.py:310
  216.8 40.0 %copy-start.8 = (bf16[128,2048]{1,0:T(8,128)(2,1)S(1)}, bf16[128,2048]{1,0:T(8,128)(2,1)}, u32[]{:S(2)}) copy-start(bf16[128,2048]{1,0:T(8,128)(2,1)} %param.43) | copy-start | bytes 1572868
  216.8 63.6 %reduce-scatter.2.cloned.1.call-start = ((), (), s32[]{:S(2)}) async-start(), calls=%async_computation.4 | async-start | bytes 655360 | tf_op jit(solution)/shard_map/reduce_scatter | solution.py:324
Sparse Core Ops, SparseCore 0:
  8.9 37.2 all-gather.1
  259.7 20.7 reduce-scatter.1
where the time goes:
time: 290 us; the launch traced here: 289 us
  blocking collectives  121 us (42%)
  waiting for transfers between devices  52.2 us (18%)
  matrix products  44.1 us (15%)
  local copies, waits for them, and re-layouts  40.9 us (14%)
  between operations  14.1 us (5%)
  other arithmetic  11.9 us (4%)
  starting transfers between devices  4.69 us (2%)
    all_gather x2, blocking collectives, entering_2(): everything = jax.tree.map(lambda part: lax.all_gather(part, axis), array)  71.7 us
    all_to_all x1, blocking collectives, per_device(): lax.all_to_all(outgoing, 'sp', split_axis=0, concat_axis=0, tiled=True)  43.2 us
    all_to_all x1, waiting for transfers between devices, per_device(): lax.all_to_all(answer.reshape(source_count, item_count, feature_count), '...  30.5 us
    reduce_scatter x1, waiting for transfers between devices, per_device(): lax.psum_scatter((routed + shared_out).astype(jnp.bfloat16), 'tp', scatte...  20.9 us
    dot_general x9, matrix products, compose(): jnp.matmul(former[1], latter[0], precision=HIGHEST) + latter[1]  11.3 us
    dynamic_slice x16, local copies, waits for them, and re-layouts, hop(): new = combine(before, jax.tree.map(lambda part: part[k], everything))  8.1 us
    dot_general x2, matrix products, expert_apply(): return jnp.dot(hidden, down_weight, preferred_element_type=jnp.float32)  7.84 us
    gather x3, local copies, waits for them, and re-layouts, per_device(): within = jnp.take_along_axis(earlier, target, axis=1)  7.24 us
  transfers between devices with their start and end apart: 3, of which 2 were waited for; matrix products, arithmetic and copies ran while one was open for 26% of the time, Pallas kernels for 0%

commit v1 on v0

v1 whole, which is shorter than its diff:
```python
import functools

import jax
import jax.numpy as jnp
from jax import lax
from jax.experimental import pallas as pl
from jax.experimental.pallas import tpu as pltpu
from jax.sharding import PartitionSpec as P

CHANNEL_SPAN = 64


NORM_EPS = 1e-06
GROUP_EPS = 0.00064
HIGHEST = lax.Precision.HIGHEST
STATE_TYPE = jnp.bfloat16

MESH = pl.DeviceIdType.MESH
VMEM_LIMIT = 60 * 1024 * 1024


def dot_nn(a, b):
    return lax.dot_general(
        a, b, (((1,), (0,)), ((), ())), precision=HIGHEST, preferred_element_type=jnp.float32
    )


def dot_nt(a, b):
    return lax.dot_general(
        a, b, (((1,), (1,)), ((), ())), precision=HIGHEST, preferred_element_type=jnp.float32
    )


def head_ones(width):
    row = lax.broadcasted_iota(jnp.int32, (width, width), 0) // CHANNEL_SPAN
    col = lax.broadcasted_iota(jnp.int32, (width, width), 1) // CHANNEL_SPAN
    return row == col


def memory_kernel(
    n_sp,
    n_tp,
    r_ref,
    k_ref,
    v_ref,
    d_ref,
    c_ref,
    g_ref,
    mix_ref,
    dcf_ref,
    gain_ref,
    bias_ref,
    w_ref,
    res_ref,
    ng_ref,
    mid_ref,
    nrm_ref,
    wbuf,
    outbox,
    inbox,
    heads,
    w_send,
    w_recv,
    f_send,
    f_recv,
    s_send,
    s_recv,
    h_send,
    h_recv,
    own_sem,
    kept,
    state,
):
    me, t = lax.axis_index("sp"), lax.axis_index("tp")
    tokens, width = r_ref.shape
    pair = 2 * CHANNEL_SPAN
    pairs = width // pair
    partner = t + 1 - 2 * lax.rem(t, 2)
    barrier = pltpu.get_barrier_semaphore()

    def greet_sp(i, carry):
        pl.semaphore_signal(
            barrier, inc=1, device_id={"sp": lax.rem(me + i, n_sp)}, device_id_type=MESH
        )
        return carry

    lax.fori_loop(1, n_sp, greet_sp, 0)
    for i in range(1, n_tp):
        pl.semaphore_signal(
            barrier, inc=1, device_id={"tp": lax.rem(t + i, n_tp)}, device_id_type=MESH
        )
    pl.semaphore_wait(barrier, n_sp - 1 + n_tp - 1)

    own = pltpu.make_async_copy(w_ref, wbuf.at[t], own_sem)
    own.start()
    w_copies = []
    for j in range(n_tp // 2):
        dest = partner if j == 0 else lax.rem(t + 2 * j, n_tp)
        copy = pltpu.make_async_remote_copy(
            src_ref=w_ref,
            dst_ref=wbuf.at[t],
            send_sem=w_send.at[j],
            recv_sem=w_recv.at[j],
            device_id={"tp": dest},
            device_id_type=MESH,
        )
        copy.start()
        w_copies.append(copy)

    f32 = jnp.float32
    row = lax.broadcasted_iota(jnp.int32, (tokens, tokens), 0)
    col = lax.broadcasted_iota(jnp.int32, (tokens, tokens), 1)
    strict = row > col
    inclusive = row >= col
    tri = jnp.where(inclusive, 1.0, 0.0).astype(f32)
    blk = head_ones(pair)
    ones_blk = jnp.where(blk, 1.0, 0.0).astype(f32)
    eye = jnp.where(
        lax.broadcasted_iota(jnp.int32, (pair, pair), 0)
        == lax.broadcasted_iota(jnp.int32, (pair, pair), 1),
        1.0,
        0.0,
    ).astype(f32)
    eye_tok = jnp.where(row == col, 1.0, 0.0).astype(f32)
    lane_head = lax.broadcasted_iota(jnp.int32, (1, pair), 1) // CHANNEL_SPAN
    lane_masks = [jnp.where(lane_head == h, 1.0, 0.0).astype(f32) for h in range(2)]

    for p in range(pairs):
        cols = pl.ds(p * pair, pair)
        recept = r_ref[:, cols].astype(f32)
        key = k_ref[:, cols].astype(f32)
        val = v_ref[:, cols].astype(f32)
        learning = 1.0 / (1.0 + jnp.exp(-c_ref[:, cols].astype(f32)))
        length = jnp.sqrt(dot_nn(key * key, ones_blk))
        unit = key / jnp.maximum(length, 1.0)
        mixed = key * (1.0 + (learning - 1.0) * mix_ref[:, cols])
        log_decay = -0.6065306597126334 / (1.0 + jnp.exp(-d_ref[:, cols].astype(f32)))
        cumulative = dot_nn(tri, log_decay)
        before = -jnp.exp(cumulative - log_decay) * unit
        inverse_decay = jnp.exp(-cumulative)
        erase = inverse_decay * unit * learning
        write = inverse_decay * mixed
        read = jnp.exp(cumulative) * recept
        removed = jnp.zeros((tokens, pair), f32)
        carried = jnp.zeros((tokens, pair), f32)
        pairs_re = []
        pairs_rw = []
        right = jnp.concatenate([erase, write], axis=0)
        for h in range(2):
            left = jnp.concatenate([before * lane_masks[h], read * lane_masks[h]], axis=0)
            prods = dot_nt(left, right)
            erase_pairs = jnp.where(strict, prods[:tokens, :tokens], 0.0)
            write_pairs = jnp.where(strict, prods[:tokens, tokens:], 0.0)
            pairs_re.append(jnp.where(inclusive, prods[tokens:, :tokens], 0.0))
            pairs_rw.append(jnp.where(inclusive, prods[tokens:, tokens:], 0.0))
            inverse = eye_tok + jnp.where(row // 2 == col // 2, erase_pairs, 0.0)
            block = 2
            while block < tokens:
                step = jnp.where(
                    (row // (2 * block) == col // (2 * block)) & (row // block != col // block),
                    erase_pairs,
                    0.0,
                )
                inverse = inverse + dot_nn(dot_nn(inverse, step), inverse)
                block *= 2
            rhs = jnp.concatenate([dot_nn(write_pairs, val), before], axis=1)
            solved = dot_nn(inverse, rhs)
            removed = removed + lane_masks[h] * solved[:, :pair]
            carried = carried + lane_masks[h] * solved[:, pair:]
        local_out = jnp.zeros((tokens, pair), f32)
        query = read
        both = jnp.concatenate([removed, carried], axis=1)
        for h in range(2):
            got = dot_nn(pairs_re[h], both)
            local_out = local_out + lane_masks[h] * (got[:, :pair] + dot_nn(pairs_rw[h], val))
            query = query + lane_masks[h] * got[:, pair:]
        final_decay = jnp.exp(cumulative[tokens - 1 : tokens, :])
        erase_end = final_decay * erase
        write_end = final_decay * write
        transit = jnp.where(blk, dot_nn(carried.T, erase_end), 0.0) + eye * final_decay
        contrib = jnp.where(
            blk, dot_nn(removed.T, erase_end) + dot_nn(val.T, write_end), 0.0
        )
        for at, full in ((0, transit), (1, contrib)):
            outbox[2 * p + at] = (full[:CHANNEL_SPAN] + full[CHANNEL_SPAN:]).astype(outbox.dtype)
        bonus = dot_nn(recept * mixed * dcf_ref[:, cols], ones_blk) * val
        kept[p, 0] = local_out
        kept[p, 1] = query
        kept[p, 2] = bonus
        state[p] = jnp.zeros((pair, pair), f32)

    def message(i):
        return pltpu.make_async_remote_copy(
            src_ref=outbox,
            dst_ref=inbox.at[me],
            send_sem=s_send.at[i],
            recv_sem=s_recv.at[me],
            device_id={"sp": i},
            device_id_type=MESH,
        )

    def send(i, carry):
        message(i).start()
        return carry

    lax.fori_loop(me + 1, n_sp, send, 0)

    def unpack(part):
        part = part.astype(f32)
        return jnp.concatenate([part * lane_masks[0], part * lane_masks[1]], axis=0)

    def hop(i, carry):
        pltpu.make_async_remote_copy(
            src_ref=outbox,
            dst_ref=inbox.at[i],
            send_sem=s_send.at[i],
            recv_sem=s_recv.at[i],
            device_id={"sp": i},
            device_id_type=MESH,
        ).wait_recv()
        for p in range(pairs):
            state[p] = dot_nn(state[p], unpack(inbox[i, 2 * p])) + unpack(inbox[i, 2 * p + 1])
        return carry

    lax.fori_loop(0, me, hop, 0)

    for p in range(pairs):
        cols = pl.ds(p * pair, pair)
        readout = kept[p, 0] + dot_nt(kept[p, 1], state[p])
        centred = readout - dot_nn(readout, ones_blk) * (1.0 / CHANNEL_SPAN)
        variance = dot_nn(centred * centred, ones_blk) * (1.0 / CHANNEL_SPAN)
        grouped = centred * lax.rsqrt(variance + GROUP_EPS) * gain_ref[:, cols] + bias_ref[:, cols]
        heads[t, :, cols] = ((grouped + kept[p, 2]) * g_ref[:, cols].astype(f32)).astype(jnp.bfloat16)

    h_copies = []
    for i in range(1, n_tp):
        copy = pltpu.make_async_remote_copy(
            src_ref=heads.at[t],
            dst_ref=heads.at[t],
            send_sem=h_send.at[i],
            recv_sem=h_recv.at[i],
            device_id={"tp": lax.rem(t + i, n_tp)},
            device_id_type=MESH,
        )
        copy.start()
        h_copies.append(copy)
    f_copies = []
    for j in range(1, n_tp // 2):
        w_copies[j].wait()
        source = lax.rem(t + n_tp - 2 * j, n_tp)
        copy = pltpu.make_async_remote_copy(
            src_ref=wbuf.at[source],
            dst_ref=wbuf.at[source],
            send_sem=f_send.at[j],
            recv_sem=f_recv.at[j],
            device_id={"tp": partner},
            device_id_type=MESH,
        )
        copy.start()
        f_copies.append(copy)
    own.wait()
    w_copies[0].wait()
    for copy in h_copies:
        copy.wait()
    for copy in f_copies:
        copy.wait()

    def drain(i, carry):
        message(i).wait_send()
        return carry

    lax.fori_loop(me + 1, n_sp, drain, 0)

    model = mid_ref.shape[1]
    whole = jnp.concatenate([heads[i] for i in range(n_tp)], axis=1)
    tile = min(512, model)
    square = jnp.zeros((tokens, 1), f32)
    for at in range(0, model, tile):
        wcol = jnp.concatenate([wbuf[i, :, at : at + tile] for i in range(n_tp)], axis=0)
        projected = jnp.dot(whole, wcol, preferred_element_type=f32)
        middle = (res_ref[:, at : at + tile].astype(f32) + projected).astype(jnp.bfloat16)
        mid_ref[:, at : at + tile] = middle
        wide = middle.astype(f32)
        square = square + jnp.sum(wide * wide, axis=1, keepdims=True)
    scale = lax.rsqrt(square * (1.0 / model) + NORM_EPS)
    for at in range(0, model, tile):
        wide = mid_ref[:, at : at + tile].astype(f32)
        nrm_ref[:, at : at + tile] = (wide * scale * ng_ref[:, at : at + tile]).astype(
            jnp.bfloat16
        )


def memory_and_norm(args):
    n_sp, n_tp = lax.axis_size("sp"), lax.axis_size("tp")
    r, k, v, d, c, g, mix, dcf, gain, bias, w, res, ng = args
    tokens, width = r.shape
    model = w.shape[1]
    pairs = width // (2 * CHANNEL_SPAN)
    dma = pltpu.SemaphoreType.DMA
    vm = pl.BlockSpec(memory_space=pltpu.VMEM)
    return pl.pallas_call(
        functools.partial(memory_kernel, n_sp, n_tp),
        out_shape=[jax.ShapeDtypeStruct((tokens, model), jnp.bfloat16)] * 2,
        in_specs=[vm] * 13,
        out_specs=[vm] * 2,
        scratch_shapes=[
            pltpu.VMEM((n_tp,) + w.shape, w.dtype),
            pltpu.VMEM((2 * pairs, CHANNEL_SPAN, 2 * CHANNEL_SPAN), STATE_TYPE),
            pltpu.VMEM((n_sp, 2 * pairs, CHANNEL_SPAN, 2 * CHANNEL_SPAN), STATE_TYPE),
            pltpu.VMEM((n_tp, tokens, width), jnp.bfloat16),
            dma((n_tp // 2,)),
            dma((n_tp // 2,)),
            dma((n_tp // 2,)),
            dma((n_tp // 2,)),
            dma((n_sp,)),
            dma((n_sp,)),
            dma((n_tp,)),
            dma((n_tp,)),
            dma,
            pltpu.VMEM((pairs, 3, tokens, 2 * CHANNEL_SPAN), jnp.float32),
            pltpu.VMEM((pairs, 2 * CHANNEL_SPAN, 2 * CHANNEL_SPAN), jnp.float32),
        ],
        compiler_params=pltpu.CompilerParams(
            collective_id=0, has_side_effects=True, vmem_limit_bytes=VMEM_LIMIT
        ),
        name="memory_and_norm",
    )(
        r, k, v, d, c, g,
        mix.reshape(1, -1), dcf.reshape(1, -1), gain.reshape(1, -1), bias.reshape(1, -1),
        w, res, ng.reshape(1, -1),
    )


def expert_apply(rows_in, gate_weight, up_weight, down_weight):
    gate_part = jnp.dot(rows_in, gate_weight, preferred_element_type=jnp.float32)
    up_part = jnp.dot(rows_in, up_weight, preferred_element_type=jnp.float32)
    hidden = (jax.nn.silu(gate_part) * up_part).astype(jnp.bfloat16)
    return jnp.dot(hidden, down_weight, preferred_element_type=jnp.float32)


def per_device(
    receptance,
    key_by_head,
    value_head_rows,
    decay_preact,
    correction_preact,
    result_sigmoid_factor,
    key_rate_mixing,
    diagonal_current_factor,
    per_head_gain,
    per_head_bias,
    output_matrix,
    residual,
    expert_norm_gain,
    routes,
    chosen_expert_weight,
    routed_gate_weight,
    routed_up_weight,
    routed_down_weight,
    common_gate_weight,
    common_up_weight,
    common_down_weight,
):
    middle, normed = memory_and_norm(
        (
            receptance,
            key_by_head,
            value_head_rows,
            decay_preact,
            correction_preact,
            result_sigmoid_factor,
            key_rate_mixing,
            diagonal_current_factor,
            per_head_gain,
            per_head_bias,
            output_matrix,
            residual,
            expert_norm_gain,
        )
    )
    tp_index = lax.axis_index("tp")
    tp_count = lax.axis_size("tp")
    sp_count = lax.axis_size("sp")
    token_count, top_count = routes.shape
    model_width = normed.shape[1]
    capacity = 3 * token_count * top_count // (2 * sp_count * tp_count)
    owned_routes = routes % tp_count == tp_index
    target = routes // tp_count
    places = jnp.arange(sp_count, dtype=jnp.int32)
    hit_counts = jnp.sum(
        jnp.where(owned_routes[:, :, None] & (target[:, :, None] == places[None, None, :]), 1, 0),
        axis=1,
    ).astype(jnp.int32)
    earlier = jnp.cumsum(hit_counts, axis=0) - hit_counts
    within = jnp.take_along_axis(earlier, target, axis=1)
    slot_index = target * capacity + within
    dropped = sp_count * capacity
    flat_slots = jnp.where(owned_routes, slot_index, dropped).reshape(-1)
    token_ids = jnp.broadcast_to(jnp.arange(token_count, dtype=jnp.int32)[:, None], routes.shape)
    slot_tokens = (
        jnp.full((dropped,), token_count, jnp.int32)
        .at[flat_slots]
        .set(token_ids.reshape(-1), mode="drop")
    )
    slot_weights = (
        jnp.zeros((dropped,), jnp.float32)
        .at[flat_slots]
        .set(chosen_expert_weight.reshape(-1), mode="drop")
    )
    padded = jnp.concatenate([normed, jnp.zeros((1, model_width), jnp.bfloat16)], axis=0)
    outgoing = padded[slot_tokens].reshape(sp_count, capacity, model_width)
    arrived = lax.all_to_all(outgoing, "sp", split_axis=0, concat_axis=0, tiled=True)
    source_count, item_count, feature_count = arrived.shape
    flat_rows = arrived.reshape(source_count * item_count, feature_count)
    answer = expert_apply(
        flat_rows, routed_gate_weight[0], routed_up_weight[0], routed_down_weight[0]
    ).astype(jnp.bfloat16)
    returned = lax.all_to_all(
        answer.reshape(source_count, item_count, feature_count),
        "sp",
        split_axis=0,
        concat_axis=0,
        tiled=True,
    )
    flat_back = returned.reshape(dropped, model_width)
    token_rows = jnp.arange(token_count, dtype=jnp.int32)
    combine_table = jnp.where(
        slot_tokens[None, :] == token_rows[:, None], slot_weights[None, :], 0.0
    )
    routed = jnp.dot(combine_table, flat_back.astype(jnp.float32), precision=HIGHEST)
    shared_out = expert_apply(normed, common_gate_weight, common_up_weight, common_down_weight)
    summed = lax.psum_scatter(
        (routed + shared_out).astype(jnp.bfloat16), "tp", scatter_dimension=1, tiled=True
    ).astype(jnp.float32)
    col_count = summed.shape[1]
    own_cols = lax.dynamic_slice_in_dim(middle, tp_index * col_count, col_count, 1)
    return (own_cols.astype(jnp.float32) + summed).astype(jnp.bfloat16)


def solution(mesh):
    return jax.shard_map(
        per_device,
        mesh=mesh,
        in_specs=(
            P("sp", "tp"),
            P("sp", "tp"),
            P("sp", "tp"),
            P("sp", "tp"),
            P("sp", "tp"),
            P("sp", "tp"),
            P("tp"),
            P("tp"),
            P("tp"),
            P("tp"),
            P("tp", None),
            P("sp", None),
            P(),
            P("sp", None),
            P("sp", None),
            P(("sp", "tp"), None, None),
            P(("sp", "tp"), None, None),
            P(("sp", "tp"), None, None),
            P(None, "tp"),
            P(None, "tp"),
            P("tp", None),
        ),
        out_specs=P("sp", "tp"),
        check_vma=False,
    )
```

time: 290 us -> 192 us (0.66)
  blocking collectives: 121 us -> 47 us
  Pallas kernels: 0 us -> 37.6 us
  matrix products: 44.1 us -> 12.5 us
  local copies, waits for them, and re-layouts: 40.9 us -> 22.8 us
  other arithmetic: 11.9 us -> 2.06 us
    all_gather x3 -> x0, blocking collectives: 77.5 us -> none  [the longest x2 71.7 us: entering_2(): everything = jax.tree.map(lambda part: lax.all_gather(part, axis), array)]
    pallas_call x0 -> x1, Pallas kernels: none -> 37.6 us  [memory_and_norm(): pl.pallas_call(functools.partial(memory_kernel, n_sp, n_tp), out_shape=[j...]
    dot_general x35 -> x0, matrix products: 30.6 us -> none  [the longest x9 11.3 us: compose(): jnp.matmul(former[1], latter[0], precision=HIGHEST) + latter[1]]
    dynamic_slice x16 -> x0, local copies, waits for them, and re-layouts: 8.1 us -> none  [hop(): new = combine(before, jax.tree.map(lambda part: part[k], everything))]
    all_to_all x1, blocking collectives: 43.2 us -> 47 us  [per_device(): lax.all_to_all(outgoing, 'sp', split_axis=0, concat_axis=0, tiled=True)]
    another operation x4 -> x0, local copies, waits for them, and re-layouts: 3.66 us -> none  [the longest x3 2.84 us: to_blocks(): source.reshape(row_count // span_len, span_len, head_count, head_size)]
    add x2 -> x0, other arithmetic: 3.28 us -> none  [memory_heads(): inner_p, inner_c = lax.associative_scan(compose, (transit, contrib), axis=0)]
  transfers between devices with their start and end apart: 3 -> 2, of which waited for: 2 -> 2; matrix products, arithmetic and copies ran while one was open for 26% -> 2% of each run, Pallas kernels for 0% -> 0%
where the time goes in v1:
time: 192 us
  waiting for transfers between devices  51.9 us (27%)
  blocking collectives  47 us (24%)
  Pallas kernels  37.6 us (20%)
  local copies, waits for them, and re-layouts  22.8 us (12%)
  between operations  13.6 us (7%)
  matrix products  12.5 us (7%)
  starting transfers between devices  4.45 us (2%)
  other arithmetic  2.06 us (1%)
    all_to_all x1, blocking collectives, per_device(): lax.all_to_all(outgoing, 'sp', split_axis=0, concat_axis=0, tiled=True)  47 us
    pallas_call x1, Pallas kernels, memory_and_norm(): pl.pallas_call(functools.partial(memory_kernel, n_sp, n_tp), out_shape=[j...  37.6 us
    all_to_all x1, waiting for transfers between devices, per_device(): lax.all_to_all(answer.reshape(source_count, item_count, feature_count), '...  31.9 us
    reduce_scatter x1, waiting for transfers between devices, per_device(): lax.psum_scatter((routed + shared_out).astype(jnp.bfloat16), 'tp', scatte...  19.9 us
    dot_general x2, matrix products, expert_apply(): return jnp.dot(hidden, down_weight, preferred_element_type=jnp.float32)  7.85 us
    gather x3, local copies, waits for them, and re-layouts, per_device(): within = jnp.take_along_axis(earlier, target, axis=1)  7.24 us
    all_to_all x1, starting transfers between devices, per_device(): lax.all_to_all(answer.reshape(source_count, item_count, feature_count), '...  4.41 us
    scatter x1, local copies, waits for them, and re-layouts, per_device(): slot_tokens = jnp.full((dropped,), token_count, jnp.int32).at[flat_slots]...  4.3 us
  transfers between devices with their start and end apart: 2, of which 2 were waited for; matrix products, arithmetic and copies ran while one was open for 2% of the time, Pallas kernels for 0%

profile of v1, /device:TPU:0, one launch (start us, length us, event | category | flops | bytes accessed | tf_op | source)
XLA Modules:
  0.0 191.8 jit_solution(2654630881770001673)
XLA Ops:
  6.5 0.9 copy.29
  7.5 0.1 bitcast_or_fusion
  7.6 0.1 fusion.26
  7.7 0.1 copy.33
  7.8 0.1 copy.35
  7.9 0.2 reduce_window_sum.11
  8.0 0.1 reshape.98
  8.1 7.1 %gather_fusion.1 = s32[1024]{0:T(1024)S(1)} fusion(s32[128,8]{1,0:T(8,128)S(1)} %sub.10, s32[1024]{0:T(1024)S(1)} %reshape.98), kind=kCustom, calls=%fused_computation.1 | custom fusion | bytes 16384 | tf_op jit(solution)/shard_map/jit(take_along_axis)/gather | solution.py:395
  15.2 0.1 reshape.101
  15.3 0.1 add_select_fusion.2
  15.4 0.1 reshape.83
  15.5 0.1 reshape.108
  15.6 4.3 %scatter_custom_fusion = s32[384]{0:T(512)S(1)} fusion(s32[1024]{0:T(1024)S(1)} %bitcast.42, s32[1024]{0:T(1024)S(1)} %reshape.108, s32[]{:T(128)} %constant.62.clone.1), kind=kCustom, calls=%fused_computation.55 | custom fusion | bytes 1540 | tf_op jit(solution)/shard_map/scatter | solution.py:403
  19.9 37.6 %memory_and_norm.1 = (bf16[128,2048]{1,0:T(8,128)(2,1)}, bf16[128,2048]{1,0:T(8,128)(2,1)}) custom-call(bf16[128,256]{1,0:T(8,128)(2,1)} %r_ref.1, bf16[128,256]{1,0:T(8,128)(2,1)} %k_ref.1, bf16[128,256]{1,0:T(8,128)(2,1)} %v_ref.1, bf16[128,256]{1,0:T(8,128)(2,1)} %d_ref.1, bf16[128,256]{1,0:T(8,128)(2,1)} %c_ref.1, bf16[128,256]{1,0:T(8,128)(2,1)} %g_ref.1, ...), custom_call_target="tpu_custom_call" | custom-call | tf_op jit(solution)/shard_map/memory_and_norm/pallas_call | solution.py:301
  57.5 1.1 concatenate.3
  58.6 3.1 %gather_fusion = bf16[384,2048]{1,0:T(8,128)(2,1)} fusion(bf16[129,2048]{1,0:T(8,128)(2,1)S(1)} %concatenate.3, s32[1024]{0:T(1024)S(1)} %pad_clamp_fusion), kind=kCustom, calls=%fused_computation | custom fusion | bytes 3147264 | tf_op jit(solution)/shard_map/gather | solution.py:411
  61.7 47.0 %all_to_all.10 = bf16[8,48,2048]{2,1,0:T(8,128)(2,1)S(1)} all-to-all(bf16[8,48,2048]{2,1,0:T(8,128)(2,1)} %bitcast.37), channel_id=1, replica_groups=mesh['sp'=8,'tp'=4] {'sp'}, dimensions={0} | all-to-all | bytes 3145728 | tf_op jit(solution)/shard_map/all_to_all | solution.py:412
  108.7 1.2 copy-done.2
  109.9 1.0 fusion.4
  110.9 5.1 %convolution_convert_fusion = bf16[384,2048]{1,0:T(8,128)(2,1)} fusion(bf16[1,512,2048]{2,1,0:T(8,128)(2,1)S(1)} %copy-done, bf16[384,2048]{1,0:T(8,128)(2,1)} %bitcast.40, bf16[1,2048,512]{2,1,0:T(8,128)(2,1)} %param.37, f32[384,512]{1,0:T(8,128)S(1)} %fusion.4), kind=kOutput, calls=%fused_computation.4 | convolution fusion | flops 1612578816 | bytes 8126464 | tf_op jit(solution)/shard_map/dot_general | solution.py:338
  116.0 4.4 %all-to-all-start.1 = ((bf16[8,48,2048]{2,1,0:T(8,128)(2,1)}), bf16[8,48,2048]{2,1,0:T(8,128)(2,1)}, u32[]{:S(2)}, u32[]{:S(2)}) async-start(bf16[8,48,2048]{2,1,0:T(8,128)(2,1)} %bitcast.38), calls=%async_computation.1 | async-start | bytes 3145728 | tf_op jit(solution)/shard_map/all_to_all | solution.py:418
  120.4 0.0 reduce-scatter.2.cloned.1.call-start
  120.5 0.1 copy.37
  120.6 0.1 reshape.116
  120.7 4.3 %scatter_custom_fusion.1 = f32[384]{0:T(512)S(1)} fusion(s32[1024]{0:T(1024)S(1)} %bitcast.43, f32[1024]{0:T(1024)S(1)} %reshape.116, f32[]{:T(128)} %constant.73.clone.1), kind=kCustom, calls=%fused_computation.53 | custom fusion | bytes 1540 | tf_op jit(solution)/shard_map/scatter | solution.py:408
  125.0 0.3 fusion.43
  125.3 31.9 %all-to-all-done.1 = bf16[8,48,2048]{2,1,0:T(8,128)(2,1)} async-done(((bf16[8,48,2048]{2,1,0:T(8,128)(2,1)}), bf16[8,48,2048]{2,1,0:T(8,128)(2,1)}, u32[]{:S(2)}, u32[]{:S(2)}) %all-to-all-start.1) | async-done | bytes 1572896 | tf_op jit(solution)/shard_map/all_to_all | solution.py:418
  157.2 3.4 %fusion.21 = f32[128,2048]{1,0:T(8,128)} fusion(bf16[384,2048]{1,0:T(8,128)(2,1)} %bitcast.13, f32[384]{0:T(512)S(1)} %scatter_custom_fusion.1, s32[384]{0:T(512)S(1)} %scatter_custom_fusion), kind=kOutput, calls=%fused_computation.23 | convolution fusion | flops 1208057856 | bytes 2624512 | tf_op jit(solution)/shard_map/dot_general | solution.py:430
  160.6 2.7 %fusion = bf16[128,2048]{1,0:T(8,128)(2,1)} fusion(f32[128,2048]{1,0:T(8,128)} %fusion.21, bf16[128,2048]{1,0:T(8,128)(2,1)S(1)} %copy-done.3, bf16[128,2048]{1,0:T(8,128)(2,1)S(1)} %copy-done.1, bf16[2048,128]{1,0:T(8,128)(2,1)} %param.40, f32[128,128]{1,0:T(8,128)S(1)} %fusion.43), kind=kOutput, calls=%fused_computation.6 | convolution fusion | flops 134840320 | bytes 3211264 | tf_op jit(solution)/shard_map/dot_general | solution.py:338
  163.3 0.0 reduce-scatter.2.cloned.1.call-update
  163.4 19.9 %reduce-scatter.2.cloned.1.call-done = bf16[128,512]{1,0:T(8,128)(2,1)} async-done(((bf16[128,2048]{1,0:T(8,128)(2,1)}), bf16[128,512]{1,0:T(8,128)(2,1)}) %reduce-scatter.2.cloned.1.call-update) | async-done | bytes 131088 | tf_op jit(solution)/shard_map/reduce_scatter | solution.py:432
  183.3 1.7 add_convert_fusion
  (20 shorter events, 0.1 us)
Async XLA Ops:
  6.5 104.3 %copy-start = (bf16[1,512,2048]{2,1,0:T(8,128)(2,1)S(1)}, bf16[1,512,2048]{2,1,0:T(8,128)(2,1)}, u32[]{:S(2)}) copy-start(bf16[1,512,2048]{2,1,0:T(8,128)(2,1)} %param.38) | copy-start | bytes 6291460
  61.7 48.2 %copy-start.6 = (bf16[1,2048,512]{2,1,0:T(8,128)(2,1)S(1)}, bf16[1,2048,512]{2,1,0:T(8,128)(2,1)}, u32[]{:S(2)}) copy-start(bf16[1,2048,512]{2,1,0:T(8,128)(2,1)} %param.36) | copy-start | bytes 6291460
  108.7 1.2 copy-start.2
  116.0 4.5 %copy-start.5 = (f32[128,8]{0,1:T(8,128)S(1)}, f32[128,8]{0,1:T(8,128)}, u32[]{:S(2)}) copy-start(f32[128,8]{0,1:T(8,128)} %param.35) | copy-start | bytes 12292
  116.0 9.0 %copy-start.1 = (bf16[128,2048]{1,0:T(8,128)(2,1)S(1)}, bf16[128,2048]{1,0:T(8,128)(2,1)}, u32[]{:S(2)}) copy-start(bf16[128,2048]{1,0:T(8,128)(2,1)} %get-tuple-element.8) | copy-start | bytes 1572868
  116.0 9.0 %copy-start.4 = (bf16[2048,128]{1,0:T(8,128)(2,1)S(1)}, bf16[2048,128]{1,0:T(8,128)(2,1)}, u32[]{:S(2)}) copy-start(bf16[2048,128]{1,0:T(8,128)(2,1)} %param.39) | copy-start | bytes 1572868
  116.0 41.2 %all-to-all-start.1 = ((bf16[8,48,2048]{2,1,0:T(8,128)(2,1)}), bf16[8,48,2048]{2,1,0:T(8,128)(2,1)}, u32[]{:S(2)}, u32[]{:S(2)}) async-start(bf16[8,48,2048]{2,1,0:T(8,128)(2,1)} %bitcast.38), calls=%async_computation.1 | async-start | bytes 3145728 | tf_op jit(solution)/shard_map/all_to_all | solution.py:418
  120.4 62.9 %reduce-scatter.2.cloned.1.call-start = ((), (), s32[]{:S(2)}) async-start(), calls=%async_computation.3 | async-start | bytes 655360 | tf_op jit(solution)/shard_map/reduce_scatter | solution.py:432
  125.3 35.3 %copy-start.3 = (bf16[128,2048]{1,0:T(8,128)(2,1)S(1)}, bf16[128,2048]{1,0:T(8,128)(2,1)}, u32[]{:S(2)}) copy-start(bf16[128,2048]{1,0:T(8,128)(2,1)} %param.41) | copy-start | bytes 1572868
Sparse Core Ops, SparseCore 0:
  163.5 19.7 reduce-scatter.1

commit v2 on v1

--- a/solution.py
+++ b/solution.py
@@ -338,6 +338,397 @@
     return jnp.dot(hidden, down_weight, preferred_element_type=jnp.float32)
 
 
+def expert_kernel(
+    n_sp,
+    n_tp,
+    cap,
+    nrm_ref,
+    own_ref,
+    wt_ref,
+    gate_hbm,
+    up_hbm,
+    down_hbm,
+    cg_ref,
+    cu_ref,
+    cd_ref,
+    out_ref,
+    gate,
+    up,
+    down,
+    blocks,
+    tables,
+    shared,
+    rows_in,
+    part,
+    core_in,
+    y_out,
+    y_in,
+    kept,
+    x_out,
+    x_in,
+    z_out,
+    z_in,
+    w_sem,
+    t_send,
+    t_recv,
+    az_send,
+    az_recv,
+    ax_send,
+    ax_recv,
+    ay_send,
+    ay_recv,
+    ac_send,
+    ac_recv,
+    rc_send,
+    rc_recv,
+    ry_send,
+    ry_recv,
+    rx_send,
+    rx_recv,
+    rz_send,
+    rz_recv,
+):
+    f32, bf16 = jnp.float32, jnp.bfloat16
+    me, t = lax.axis_index("sp"), lax.axis_index("tp")
+    tokens, model = nrm_ref.shape
+    groups = n_sp // 2
+    fars = n_tp // 2
+    strip = tokens // n_tp
+    cols = model // n_tp
+    core_to = t + 1 - 2 * lax.rem(t, 2)
+    x_to = me + 1 - 2 * lax.rem(me, 2)
+    parity = lax.rem(t, 2)
+
+    def remote(src, dst, send, recv, device):
+        return pltpu.make_async_remote_copy(
+            src_ref=src,
+            dst_ref=dst,
+            send_sem=send,
+            recv_sem=recv,
+            device_id=device,
+            device_id_type=MESH,
+        )
+
+    barrier = pltpu.get_barrier_semaphore()
+
+    def greet(i, carry):
+        pl.semaphore_signal(
+            barrier, inc=1, device_id={"sp": lax.rem(me + i, n_sp)}, device_id_type=MESH
+        )
+        return carry
+
+    lax.fori_loop(1, n_sp, greet, 0)
+    for i in range(1, n_tp):
+        pl.semaphore_signal(
+            barrier, inc=1, device_id={"tp": lax.rem(t + i, n_tp)}, device_id_type=MESH
+        )
+    loads = [
+        pltpu.make_async_copy(src, dst, w_sem.at[i])
+        for i, (src, dst) in enumerate(((gate_hbm, gate), (up_hbm, up), (down_hbm, down)))
+    ]
+    for load in loads:
+        load.start()
+    pl.semaphore_wait(barrier, n_sp - 1 + n_tp - 1)
+
+    def source(j):
+        return lax.rem(me + n_sp - 2 * j, n_sp)
+
+    def near(b):
+        return b + 1 - 2 * lax.rem(b, 2)
+
+    def rows(b, q):
+        return blocks.at[b, pl.ds(pl.multiple_of(q * strip, strip), strip)]
+
+    def own_rows():
+        return nrm_ref.at[pl.ds(pl.multiple_of(t * strip, strip), strip)]
+
+    def table_copy(i):
+        to = lax.rem(me + i, n_sp)
+        return remote(wt_ref.at[to], tables.at[me], t_send.at[i], t_recv.at[i], {"sp": to})
+
+    def z_copy(j):
+        to = lax.rem(me + 2 * j, n_sp)
+        return remote(own_rows(), rows(me, t), az_send.at[j], az_recv.at[j], {"sp": to})
+
+    for i in range(1, n_sp):
+        table_copy(i).start()
+    blocks[me] = nrm_ref[...]
+    tables[me] = wt_ref[me]
+
+    def x_own():
+        return remote(own_rows(), rows(me, t), ax_send.at[0], ax_recv.at[0], {"sp": x_to})
+
+    def x_copy(j):
+        b = source(j)
+        return remote(rows(b, t), rows(b, t), ax_send.at[j], ax_recv.at[j], {"sp": x_to})
+
+    def tp_copies(j, side):
+        b = source(j) if side == 0 else near(source(j))
+        return [
+            remote(
+                rows(b, t),
+                rows(b, t),
+                ay_send.at[j, side, k],
+                ay_recv.at[j, side, k],
+                {"tp": lax.rem(t + 2 * k, n_tp)},
+            )
+            for k in range(1, fars)
+        ]
+
+    def core_copies(j, side):
+        b = source(j) if side == 0 else near(source(j))
+        found = []
+        for k in range(fars):
+            q = lax.rem(t + n_tp - 2 * k, n_tp)
+            found.append(
+                remote(
+                    rows(b, q),
+                    rows(b, q),
+                    ac_send.at[j, side, k],
+                    ac_recv.at[j, side, k],
+                    {"tp": core_to},
+                )
+            )
+        return found
+
+    x_own().start()
+    for j in range(1, groups):
+        z_copy(j).start()
+
+    hid = jnp.dot(nrm_ref[...], cg_ref[...], preferred_element_type=f32)
+    hid = hid / (1.0 + jnp.exp(-hid)) * jnp.dot(
+        nrm_ref[...], cu_ref[...], preferred_element_type=f32
+    )
+    hid = hid.astype(bf16)
+    for q in range(n_tp):
+        shared[q] = jnp.dot(
+            hid, cd_ref[:, q * cols : (q + 1) * cols], preferred_element_type=f32
+        )
+    for load in loads:
+        load.wait()
+
+    slot_row = lax.broadcasted_iota(jnp.int32, (cap, tokens), 0).astype(f32)
+    earlier = jnp.where(
+        lax.broadcasted_iota(jnp.int32, (tokens, tokens), 0)
+        < lax.broadcasted_iota(jnp.int32, (tokens, tokens), 1),
+        1.0,
+        0.0,
+    ).astype(bf16)
+
+    def rc_copy(j, m):
+        q = 2 * m + (1 - parity)
+        return remote(
+            part.at[j, q], core_in.at[j, m], rc_send.at[j, m], rc_recv.at[j, m], {"tp": core_to}
+        )
+
+    def ry_copy(j, k):
+        return remote(
+            y_out.at[j, k],
+            y_in.at[j, k],
+            ry_send.at[j, k],
+            ry_recv.at[j, k],
+            {"tp": lax.rem(t + 2 * k, n_tp)},
+        )
+
+    def rx_copy(j):
+        return remote(x_out.at[j], x_in.at[j], rx_send.at[j], rx_recv.at[j], {"sp": x_to})
+
+    def rz_copy(j):
+        return remote(
+            z_out.at[j], z_in.at[j], rz_send.at[j], rz_recv.at[j], {"sp": source(j)}
+        )
+
+    def z_stage(j):
+        @pl.when(j > 0)
+        def _():
+            z_copy(j).wait_recv()
+            x_copy(j).start()
+            for copy in tp_copies(j, 0):
+                copy.start()
+
+    def x_stage(j):
+        x_copy(j).wait_recv()
+        for copy in tp_copies(j, 1):
+            copy.start()
+
+    def y_stage(j):
+        @pl.when(j > 0)
+        def _():
+            for copy in tp_copies(j, 0):
+                copy.wait_recv()
+            for copy in core_copies(j, 0):
+                copy.start()
+
+        for copy in tp_copies(j, 1):
+            copy.wait_recv()
+        for copy in core_copies(j, 1):
+            copy.start()
+
+    def compute(j):
+        @pl.when(j > 0)
+        def _():
+            for copy in core_copies(j, 0):
+                copy.wait_recv()
+            table_copy(2 * j).wait_recv()
+
+        for copy in core_copies(j, 1):
+            copy.wait_recv()
+        b0 = source(j)
+        b1 = near(b0)
+        table_copy(lax.rem(me + n_sp - b1, n_sp)).wait_recv()
+        weighted = []
+        for side, b in ((0, b0), (1, b1)):
+            w = tables[b]
+            routed = jnp.where(w > 0.0, 1.0, 0.0).astype(bf16)
+            rank = jnp.dot(routed, earlier, preferred_element_type=f32)
+            hit = (slot_row == rank[0:1, :]) & (w[0:1, :] > 0.0)
+            pick = jnp.where(hit, 1.0, 0.0).astype(bf16)
+            full = jnp.where(hit, w[0:1, :], 0.0).T
+            high = full.astype(bf16)
+            low = (full - high.astype(f32)).astype(bf16)
+            weighted.append((high, low))
+            for q in range(n_tp):
+                at = slice(q * cols, (q + 1) * cols)
+                rows_in[side * cap : (side + 1) * cap, at] = jnp.dot(
+                    pick, blocks[b, :, at], preferred_element_type=f32
+                ).astype(bf16)
+        x = rows_in[...]
+        g = jnp.dot(x, gate[0], preferred_element_type=f32)
+        u = jnp.dot(x, up[0], preferred_element_type=f32)
+        hidden = (g / (1.0 + jnp.exp(-g)) * u).astype(bf16)
+        first = jnp.where(j == 0, 1.0, 0.0).astype(f32)
+        for q in range(n_tp):
+            answer = jnp.dot(
+                hidden, down[0, :, q * cols : (q + 1) * cols], preferred_element_type=f32
+            ).astype(bf16)
+            for side in range(2):
+                high, low = weighted[side]
+                a = answer[side * cap : (side + 1) * cap]
+                total = jnp.dot(high, a, preferred_element_type=f32) + jnp.dot(
+                    low, a, preferred_element_type=f32
+                )
+                if side == 0:
+                    total = total + first * shared[q]
+                part[j, q, side * tokens : (side + 1) * tokens] = total.astype(bf16)
+        for m in range(fars):
+            rc_copy(j, m).start()
+
+    def core_stage(j):
+        for m in range(fars):
+            rc_copy(j, m).wait_recv()
+        for k in range(1, fars):
+            q = lax.rem(t + 2 * k, n_tp)
+            y_out[j, k] = (
+                part[j, q].astype(f32) + core_in[j, lax.div(q, 2)].astype(f32)
+            ).astype(bf16)
+            ry_copy(j, k).start()
+
+    def y_reduce(j):
+        for k in range(1, fars):
+            ry_copy(j, k).wait_recv()
+        for side in (1, 0):
+            at = slice(side * tokens, (side + 1) * tokens)
+            total = part[j, t, at].astype(f32) + core_in[j, lax.div(t, 2), at].astype(f32)
+            for k in range(1, fars):
+                total = total + y_in[j, k, at].astype(f32)
+            if side == 1:
+                x_out[j] = total.astype(bf16)
+                rx_copy(j).start()
+            else:
+                kept[j] = total
+
+    def x_reduce(j):
+        rx_copy(j).wait_recv()
+        kept[j] = kept[j] + x_in[j].astype(f32)
+
+        @pl.when(j > 0)
+        def _():
+            z_out[j] = kept[j].astype(bf16)
+            rz_copy(j).start()
+
+    stages = (x_reduce, y_reduce, core_stage, compute, y_stage, x_stage, z_stage)
+    lags = (6, 5, 4, 3, 2, 1, 0)
+
+    def step(s, carry):
+        for lag, stage in sorted(zip(lags, stages), key=lambda pair: pair[0]):
+
+            @pl.when((s >= lag) & (s < groups + lag))
+            def _():
+                stage(s - lag)
+
+        return carry
+
+    lax.fori_loop(0, groups + lags[0], step, 0)
+
+    total = kept[0] + own_ref[...].astype(f32)
+    for j in range(1, groups):
+        rz_copy(j).wait_recv()
+        total = total + z_in[j].astype(f32)
+    out_ref[...] = total.astype(out_ref.dtype)
+
+    for i in range(1, n_sp):
+        table_copy(i).wait_send()
+    x_own().wait_send()
+    for j in range(groups):
+        if j > 0:
+            z_copy(j).wait_send()
+            x_copy(j).wait_send()
+            rz_copy(j).wait_send()
+        for side in range(2):
+            if j > 0 or side > 0:
+                for copy in tp_copies(j, side) + core_copies(j, side):
+                    copy.wait_send()
+        for m in range(fars):
+            rc_copy(j, m).wait_send()
+        for k in range(1, fars):
+            ry_copy(j, k).wait_send()
+        rx_copy(j).wait_send()
+
+
+def expert_layer(normed, own_cols, weights, gate, up, down, cgate, cup, cdown, cap):
+    n_sp, n_tp = lax.axis_size("sp"), lax.axis_size("tp")
+    tokens, model = normed.shape
+    groups, fars, cols = n_sp // 2, n_tp // 2, model // n_tp
+    bf16, f32 = jnp.bfloat16, jnp.float32
+    dma = pltpu.SemaphoreType.DMA
+    vm = pl.BlockSpec(memory_space=pltpu.VMEM)
+    hbm = pl.BlockSpec(memory_space=pl.ANY)
+    pairs = [dma((n_sp,)), dma((n_sp,)), dma((groups,)), dma((groups,)), dma((groups,)), dma((groups,))]
+    pairs += [dma((groups, 2, fars))] * 4
+    pairs += [dma((groups, fars))] * 4
+    pairs += [dma((groups,))] * 4
+    return pl.pallas_call(
+        functools.partial(expert_kernel, n_sp, n_tp, cap),
+        out_shape=jax.ShapeDtypeStruct((tokens, cols), bf16),
+        in_specs=[vm, vm, vm, hbm, hbm, hbm, vm, vm, vm],
+        out_specs=vm,
+        scratch_shapes=[
+            pltpu.VMEM(gate.shape, bf16),
+            pltpu.VMEM(up.shape, bf16),
+            pltpu.VMEM(down.shape, bf16),
+            pltpu.VMEM((n_sp, tokens, model), bf16),
+            pltpu.VMEM(weights.shape, f32),
+            pltpu.VMEM((n_tp, tokens, cols), f32),
+            pltpu.VMEM((2 * cap, model), bf16),
+            pltpu.VMEM((groups, n_tp, 2 * tokens, cols), bf16),
+            pltpu.VMEM((groups, fars, 2 * tokens, cols), bf16),
+            pltpu.VMEM((groups, fars, 2 * tokens, cols), bf16),
+            pltpu.VMEM((groups, fars, 2 * tokens, cols), bf16),
+            pltpu.VMEM((groups, tokens, cols), f32),
+            pltpu.VMEM((groups, tokens, cols), bf16),
+            pltpu.VMEM((groups, tokens, cols), bf16),
+            pltpu.VMEM((groups, tokens, cols), bf16),
+            pltpu.VMEM((groups, tokens, cols), bf16),
+            dma((3,)),
+        ]
+        + pairs,
+        compiler_params=pltpu.CompilerParams(
+            collective_id=1, has_side_effects=True, vmem_limit_bytes=VMEM_LIMIT
+        ),
+        name="expert_layer",
+    )(normed, own_cols, weights, gate, up, down, cgate, cup, cdown)
+
+
 def per_device(
     receptance,
     key_by_head,
@@ -384,6 +775,26 @@
     token_count, top_count = routes.shape
     model_width = normed.shape[1]
     capacity = 3 * token_count * top_count // (2 * sp_count * tp_count)
+    held = sp_count * token_count * model_width * normed.dtype.itemsize
+    if sp_count % 2 == 0 and tp_count % 2 == 0 and 6 * held <= VMEM_LIMIT:
+        mine = jnp.arange(sp_count, dtype=jnp.int32) * tp_count + tp_index
+        named = routes.T[None, :, :] == mine[:, None, None]
+        weights = jnp.sum(jnp.where(named, chosen_expert_weight.T[None, :, :], 0.0), axis=1)
+        weights = jnp.broadcast_to(weights[:, None, :], (sp_count, 8, token_count))
+        col_count = model_width // tp_count
+        own_cols = lax.dynamic_slice_in_dim(middle, tp_index * col_count, col_count, 1)
+        return expert_layer(
+            normed,
+            own_cols,
+            weights,
+            routed_gate_weight,
+            routed_up_weight,
+            routed_down_weight,
+            common_gate_weight,
+            common_up_weight,
+            common_down_weight,
+            capacity,
+        )
     owned_routes = routes % tp_count == tp_index
     target = routes // tp_count
     places = jnp.arange(sp_count, dtype=jnp.int32)

time: 192 us -> 115 us (0.60)
  Pallas kernels: 37.6 us -> 111 us
  waiting for transfers between devices: 51.9 us -> 0 us
  blocking collectives: 47 us -> 0 us
  local copies, waits for them, and re-layouts: 22.8 us -> 3.15 us
  between operations: 13.6 us -> 0.03 us
  matrix products: 12.5 us -> 0 us
  starting transfers between devices: 4.45 us -> 0 us
    pallas_call x0 -> x1, Pallas kernels: none -> 73 us  [expert_layer(): pl.pallas_call(functools.partial(expert_kernel, n_sp, n_tp, cap), out_sha...]
    all_to_all x1 -> x0, blocking collectives: 47 us -> none  [per_device(): lax.all_to_all(outgoing, 'sp', split_axis=0, concat_axis=0, tiled=True)]
    all_to_all x1 -> x0, waiting for transfers between devices: 31.9 us -> none  [per_device(): lax.all_to_all(answer.reshape(source_count, item_count, feature_count), '...]
    reduce_scatter x1 -> x0, waiting for transfers between devices: 19.9 us -> none  [per_device(): lax.psum_scatter((routed + shared_out).astype(jnp.bfloat16), 'tp', scatte...]
    dot_general x5 -> x0, matrix products: 12.5 us -> none  [the longest x2 7.85 us: expert_apply(): return jnp.dot(hidden, down_weight, preferred_element_type=jnp.float32)]
    gather x4 -> x0, local copies, waits for them, and re-layouts: 10.4 us -> none  [the longest x3 7.24 us: per_device(): within = jnp.take_along_axis(earlier, target, axis=1)]
    scatter x2 -> x0, local copies, waits for them, and re-layouts: 8.61 us -> none  [the longest x1 4.3 us: per_device(): slot_tokens = jnp.full((dropped,), token_count, jnp.int32).at[flat_slots]...]
    all_to_all x1 -> x0, starting transfers between devices: 4.41 us -> none  [per_device(): lax.all_to_all(answer.reshape(source_count, item_count, feature_count), '...]
  transfers between devices with their start and end apart: 2 -> 0, of which waited for: 2 -> 0; matrix products, arithmetic and copies ran while one was open for 2% -> 0% of each run, Pallas kernels for 0% -> 0%
where the time goes in v2:
time: 115 us; the launch traced here: 114 us
  Pallas kernels  111 us (97%)
  local copies, waits for them, and re-layouts  3.15 us (3%)
    pallas_call x1, Pallas kernels, expert_layer(): pl.pallas_call(functools.partial(expert_kernel, n_sp, n_tp, cap), out_sha...  73 us
    pallas_call x1, Pallas kernels, memory_and_norm(): pl.pallas_call(functools.partial(memory_kernel, n_sp, n_tp), out_shape=[j...  37.6 us

profile of v2, /device:TPU:0, one launch (start us, length us, event | category | flops | bytes accessed | tf_op | source)
XLA Modules:
  0.0 114.4 jit_solution(11247423470180731792)
XLA Ops:
  0.0 0.0 copy-start
  0.0 0.0 copy-start.1
  0.0 37.6 %memory_and_norm.1 = (bf16[128,2048]{1,0:T(8,128)(2,1)}, bf16[128,2048]{1,0:T(8,128)(2,1)}) custom-call(bf16[128,256]{1,0:T(8,128)(2,1)} %r_ref.1, bf16[128,256]{1,0:T(8,128)(2,1)} %k_ref.1, bf16[128,256]{1,0:T(8,128)(2,1)} %v_ref.1, bf16[128,256]{1,0:T(8,128)(2,1)} %d_ref.1, bf16[128,256]{1,0:T(8,128)(2,1)} %c_ref.1, bf16[128,256]{1,0:T(8,128)(2,1)} %g_ref.1, ...), custom_call_target="tpu_custom_call" | custom-call | tf_op jit(solution)/shard_map/memory_and_norm/pallas_call | solution.py:301
  37.6 1.6 %constant_dynamic-slice_fusion.own_ref = bf16[128,512]{1,0:T(8,128)(2,1)} fusion(bf16[128,2048]{1,0:T(8,128)(2,1)} %get-tuple-element.8, s32[]{:T(128)S(6)} %select_n.7), kind=kLoop, calls=%fused_computation.25 | loop fusion | bytes 262148 | tf_op jit(solution)/shard_map/dynamic_slice | solution.py:785
  39.1 0.0 copy-done
  39.2 0.0 copy-done.1
  39.2 0.7 fusion.wt_ref
  39.8 73.0 %expert_layer.1 = bf16[128,512]{1,0:T(8,128)(2,1)} custom-call(bf16[128,2048]{1,0:T(8,128)(2,1)} %get-tuple-element.7.nrm_ref, bf16[128,512]{1,0:T(8,128)(2,1)} %constant_dynamic-slice_fusion.own_ref, f32[8,8,128]{2,1,0:T(8,128)} %fusion.wt_ref, bf16[1,2048,512]{2,1,0:T(8,128)(2,1)} %gate_hbm.1, bf16[1,2048,512]{2,1,0:T(8,128)(2,1)} %up_hbm.1, ...), custom_call_target="tpu_custom_call" | custom-call | tf_op jit(solution)/shard_map/expert_layer/pallas_call | solution.py:700
  112.9 1.6 %copy.23 = bf16[128,512]{1,0:T(8,128)(2,1)} copy(bf16[128,512]{1,0:T(8,128)(2,1)} %expert_layer.1) | data formatting | bytes 262144
  (1 shorter events, 0.0 us)
Async XLA Ops:
  0.0 39.2 %copy-start = (f32[128,8]{0,1:T(8,128)S(1)}, f32[128,8]{0,1:T(8,128)}, u32[]{:S(2)}) copy-start(f32[128,8]{0,1:T(8,128)} %param.35) | copy-start | bytes 12292
  0.0 39.2 %copy-start.1 = (s32[128,8]{0,1:T(8,128)S(1)}, s32[128,8]{0,1:T(8,128)}, u32[]{:S(2)}) copy-start(s32[128,8]{0,1:T(8,128)} %param.34) | copy-start | bytes 12292

commit v3 on v2

--- a/solution.py
+++ b/solution.py
@@ -55,6 +55,7 @@
     ng_ref,
     mid_ref,
     nrm_ref,
+    cut_ref,
     wbuf,
     outbox,
     inbox,
@@ -282,6 +283,13 @@
         mid_ref[:, at : at + tile] = middle
         wide = middle.astype(f32)
         square = square + jnp.sum(wide * wide, axis=1, keepdims=True)
+    cut = model // n_tp
+    for i in range(n_tp):
+
+        @pl.when(t == i)
+        def _():
+            cut_ref[...] = mid_ref[:, i * cut : (i + 1) * cut]
+
     scale = lax.rsqrt(square * (1.0 / model) + NORM_EPS)
     for at in range(0, model, tile):
         wide = mid_ref[:, at : at + tile].astype(f32)
@@ -300,9 +308,10 @@
     vm = pl.BlockSpec(memory_space=pltpu.VMEM)
     return pl.pallas_call(
         functools.partial(memory_kernel, n_sp, n_tp),
-        out_shape=[jax.ShapeDtypeStruct((tokens, model), jnp.bfloat16)] * 2,
+        out_shape=[jax.ShapeDtypeStruct((tokens, model), jnp.bfloat16)] * 2
+        + [jax.ShapeDtypeStruct((tokens, model // n_tp), jnp.bfloat16)],
         in_specs=[vm] * 13,
-        out_specs=[vm] * 2,
+        out_specs=[vm] * 3,
         scratch_shapes=[
             pltpu.VMEM((n_tp,) + w.shape, w.dtype),
             pltpu.VMEM((2 * pairs, CHANNEL_SPAN, 2 * CHANNEL_SPAN), STATE_TYPE),
@@ -495,18 +504,6 @@
     for j in range(1, groups):
         z_copy(j).start()
 
-    hid = jnp.dot(nrm_ref[...], cg_ref[...], preferred_element_type=f32)
-    hid = hid / (1.0 + jnp.exp(-hid)) * jnp.dot(
-        nrm_ref[...], cu_ref[...], preferred_element_type=f32
-    )
-    hid = hid.astype(bf16)
-    for q in range(n_tp):
-        shared[q] = jnp.dot(
-            hid, cd_ref[:, q * cols : (q + 1) * cols], preferred_element_type=f32
-        )
-    for load in loads:
-        load.wait()
-
     slot_row = lax.broadcasted_iota(jnp.int32, (cap, tokens), 0).astype(f32)
     earlier = jnp.where(
         lax.broadcasted_iota(jnp.int32, (tokens, tokens), 0)
@@ -564,7 +561,22 @@
         for copy in core_copies(j, 1):
             copy.start()
 
+    def common():
+        hid = jnp.dot(nrm_ref[...], cg_ref[...], preferred_element_type=f32)
+        hid = hid / (1.0 + jnp.exp(-hid)) * jnp.dot(
+            nrm_ref[...], cu_ref[...], preferred_element_type=f32
+        )
+        hid = hid.astype(bf16)
+        for q in range(n_tp):
+            shared[q] = jnp.dot(
+                hid, cd_ref[:, q * cols : (q + 1) * cols], preferred_element_type=f32
+            )
+        for load in loads:
+            load.wait()
+
     def compute(j):
+        pl.when(j == 1 % groups)(common)
+
         @pl.when(j > 0)
         def _():
             for copy in core_copies(j, 0):
@@ -616,51 +628,64 @@
     def core_stage(j):
         for m in range(fars):
             rc_copy(j, m).wait_recv()
+        for m in range(fars):
+            q = 2 * m + parity
+            x_out[j, m] = (
+                part[j, q, tokens:].astype(f32) + core_in[j, m, tokens:].astype(f32)
+            ).astype(bf16)
+        rx_copy(j).start()
+
+    def three_terms(j, q):
+        m = lax.div(q, 2)
+        return (
+            part[j, q, :tokens].astype(f32)
+            + core_in[j, m, :tokens].astype(f32)
+            + x_in[j, m].astype(f32)
+        )
+
+    def x_reduce(j):
+        rx_copy(j).wait_recv()
         for k in range(1, fars):
-            q = lax.rem(t + 2 * k, n_tp)
-            y_out[j, k] = (
-                part[j, q].astype(f32) + core_in[j, lax.div(q, 2)].astype(f32)
-            ).astype(bf16)
+            y_out[j, k] = three_terms(j, lax.rem(t + 2 * k, n_tp)).astype(bf16)
             ry_copy(j, k).start()
 
     def y_reduce(j):
+        total = three_terms(j, t)
         for k in range(1, fars):
             ry_copy(j, k).wait_recv()
-        for side in (1, 0):
-            at = slice(side * tokens, (side + 1) * tokens)
-            total = part[j, t, at].astype(f32) + core_in[j, lax.div(t, 2), at].astype(f32)
-            for k in range(1, fars):
-                total = total + y_in[j, k, at].astype(f32)
-            if side == 1:
-                x_out[j] = total.astype(bf16)
-                rx_copy(j).start()
-            else:
-                kept[j] = total
-
-    def x_reduce(j):
-        rx_copy(j).wait_recv()
-        kept[j] = kept[j] + x_in[j].astype(f32)
+            total = total + y_in[j, k].astype(f32)
+
+        @pl.when(j == 0)
+        def _():
+            kept[...] = total
 
         @pl.when(j > 0)
         def _():
-            z_out[j] = kept[j].astype(bf16)
+            z_out[j] = total.astype(bf16)
             rz_copy(j).start()
 
-    stages = (x_reduce, y_reduce, core_stage, compute, y_stage, x_stage, z_stage)
-    lags = (6, 5, 4, 3, 2, 1, 0)
+    stages = (
+        (0, z_stage),
+        (1, x_stage),
+        (4, core_stage),
+        (5, x_reduce),
+        (6, y_reduce),
+        (3, compute),
+        (2, y_stage),
+    )
 
     def step(s, carry):
-        for lag, stage in sorted(zip(lags, stages), key=lambda pair: pair[0]):
+        for lag, stage in stages:
 
             @pl.when((s >= lag) & (s < groups + lag))
             def _():
-                stage(s - lag)
+                stage(lax.rem(s - lag + 1, groups))
 
         return carry
 
-    lax.fori_loop(0, groups + lags[0], step, 0)
-
-    total = kept[0] + own_ref[...].astype(f32)
+    lax.fori_loop(0, groups + 6, step, 0)
+
+    total = kept[...] + own_ref[...].astype(f32)
     for j in range(1, groups):
         rz_copy(j).wait_recv()
         total = total + z_in[j].astype(f32)
@@ -712,11 +737,11 @@
             pltpu.VMEM((2 * cap, model), bf16),
             pltpu.VMEM((groups, n_tp, 2 * tokens, cols), bf16),
             pltpu.VMEM((groups, fars, 2 * tokens, cols), bf16),
-            pltpu.VMEM((groups, fars, 2 * tokens, cols), bf16),
-            pltpu.VMEM((groups, fars, 2 * tokens, cols), bf16),
-            pltpu.VMEM((groups, tokens, cols), f32),
-            pltpu.VMEM((groups, tokens, cols), bf16),
-            pltpu.VMEM((groups, tokens, cols), bf16),
+            pltpu.VMEM((groups, fars, tokens, cols), bf16),
+            pltpu.VMEM((groups, fars, tokens, cols), bf16),
+            pltpu.VMEM((tokens, cols), f32),
+            pltpu.VMEM((groups, fars, tokens, cols), bf16),
+            pltpu.VMEM((groups, fars, tokens, cols), bf16),
             pltpu.VMEM((groups, tokens, cols), bf16),
             pltpu.VMEM((groups, tokens, cols), bf16),
             dma((3,)),
@@ -752,7 +777,7 @@
     common_up_weight,
     common_down_weight,
 ):
-    middle, normed = memory_and_norm(
+    middle, normed, own_cols = memory_and_norm(
         (
             receptance,
             key_by_head,
@@ -781,8 +806,6 @@
         named = routes.T[None, :, :] == mine[:, None, None]
         weights = jnp.sum(jnp.where(named, chosen_expert_weight.T[None, :, :], 0.0), axis=1)
         weights = jnp.broadcast_to(weights[:, None, :], (sp_count, 8, token_count))
-        col_count = model_width // tp_count
-        own_cols = lax.dynamic_slice_in_dim(middle, tp_index * col_count, col_count, 1)
         return expert_layer(
             normed,
             own_cols,

time: 115 us -> 110 us (0.957)
  Pallas kernels: 111 us -> 107 us
  local copies, waits for them, and re-layouts: 3.15 us -> 1.57 us
    pallas_call x1, Pallas kernels: 73 us -> 69 us  [expert_layer(): pl.pallas_call(functools.partial(expert_kernel, n_sp, n_tp, cap), out_sha...]
    dynamic_slice x1 -> x0, local copies, waits for them, and re-layouts: 1.57 us -> none  [per_device(): lax.dynamic_slice_in_dim(middle, tp_index * col_count, col_count, 1)]
where the time goes in v3:
time: 110 us
  Pallas kernels  107 us (97%)
  local copies, waits for them, and re-layouts  1.57 us (1%)
  other arithmetic  1.41 us (1%)
    pallas_call x1, Pallas kernels, expert_layer(): pl.pallas_call(functools.partial(expert_kernel, n_sp, n_tp, cap), out_sha...  69 us
    pallas_call x1, Pallas kernels, memory_and_norm(): pl.pallas_call(functools.partial(memory_kernel, n_sp, n_tp), out_shape=[j...  37.8 us

profile of v3, /device:TPU:0, one launch (start us, length us, event | category | flops | bytes accessed | tf_op | source)
XLA Modules:
  0.0 109.9 jit_solution(15358428264036349024)
XLA Ops:
  0.0 37.8 %memory_and_norm.1 = (bf16[128,2048]{1,0:T(8,128)(2,1)}, bf16[128,2048]{1,0:T(8,128)(2,1)}, bf16[128,512]{1,0:T(8,128)(2,1)}) custom-call(bf16[128,256]{1,0:T(8,128)(2,1)} %r_ref.1, bf16[128,256]{1,0:T(8,128)(2,1)} %k_ref.1, bf16[128,256]{1,0:T(8,128)(2,1)} %v_ref.1, bf16[128,256]{1,0:T(8,128)(2,1)} %d_ref.1, bf16[128,256]{1,0:T(8,128)(2,1)} %c_ref.1, ...), custom_call_target="tpu_custom_call" | custom-call | tf_op jit(solution)/shard_map/memory_and_norm/pallas_call | solution.py:309
  37.9 1.4 %fusion.wt_ref = f32[8,8,128]{2,1,0:T(8,128)} fusion(f32[8,128]{1,0:T(8,128)} %bitcast.12, s32[8,128]{1,0:T(8,128)} %bitcast.13, s32[8]{0:T(128)S(1)} %multiply_add_fusion), kind=kOutput, calls=%fused_computation | output fusion | flops 17415 | bytes 40992 | tf_op jit(solution)/shard_map/broadcast_in_dim | solution.py:808
  39.3 69.0 %expert_layer.1 = bf16[128,512]{1,0:T(8,128)(2,1)} custom-call(bf16[128,2048]{1,0:T(8,128)(2,1)} %get-tuple-element.7.nrm_ref, bf16[128,512]{1,0:T(8,128)(2,1)} %get-tuple-element.8.own_ref, f32[8,8,128]{2,1,0:T(8,128)} %fusion.wt_ref, bf16[1,2048,512]{2,1,0:T(8,128)(2,1)} %gate_hbm.1, bf16[1,2048,512]{2,1,0:T(8,128)(2,1)} %up_hbm.1, ...), custom_call_target="tpu_custom_call" | custom-call | tf_op jit(solution)/shard_map/expert_layer/pallas_call | solution.py:725
  108.3 1.6 %copy.23 = bf16[128,512]{1,0:T(8,128)(2,1)} copy(bf16[128,512]{1,0:T(8,128)(2,1)} %expert_layer.1) | data formatting | bytes 262144
  (1 shorter events, 0.0 us)

commit v4 on v3

--- a/solution.py
+++ b/solution.py
@@ -19,10 +19,21 @@
 VMEM_LIMIT = 60 * 1024 * 1024
 
 
-def dot_nn(a, b):
+def dot_full(a, b):
     return lax.dot_general(
         a, b, (((1,), (0,)), ((), ())), precision=HIGHEST, preferred_element_type=jnp.float32
     )
+
+
+def halves_of(a):
+    high = a.astype(jnp.bfloat16)
+    return high, (a - high.astype(jnp.float32)).astype(jnp.bfloat16)
+
+
+def dot_nn(a, b):
+    (ah, al), (bh, bl) = halves_of(a), halves_of(b)
+    dot = functools.partial(jnp.dot, preferred_element_type=jnp.float32)
+    return dot(ah, bh) + (dot(ah, bl) + dot(al, bh))
 
 
 def dot_nt(a, b):
@@ -136,7 +147,7 @@
         unit = key / jnp.maximum(length, 1.0)
         mixed = key * (1.0 + (learning - 1.0) * mix_ref[:, cols])
         log_decay = -0.6065306597126334 / (1.0 + jnp.exp(-d_ref[:, cols].astype(f32)))
-        cumulative = dot_nn(tri, log_decay)
+        cumulative = dot_full(tri, log_decay)
         before = -jnp.exp(cumulative - log_decay) * unit
         inverse_decay = jnp.exp(-cumulative)
         erase = inverse_decay * unit * learning
@@ -144,30 +155,29 @@
         read = jnp.exp(cumulative) * recept
         removed = jnp.zeros((tokens, pair), f32)
         carried = jnp.zeros((tokens, pair), f32)
-        pairs_re = []
-        pairs_rw = []
         right = jnp.concatenate([erase, write], axis=0)
+        prods = [
+            dot_nt(jnp.concatenate([before * mask, read * mask], axis=0), right)
+            for mask in lane_masks
+        ]
+        erase_pairs = [jnp.where(strict, part[:tokens, :tokens], 0.0) for part in prods]
+        write_pairs = [jnp.where(strict, part[:tokens, tokens:], 0.0) for part in prods]
+        pairs_re = [jnp.where(inclusive, part[tokens:, :tokens], 0.0) for part in prods]
+        pairs_rw = [jnp.where(inclusive, part[tokens:, tokens:], 0.0) for part in prods]
+        inverse = [eye_tok + jnp.where(row // 2 == col // 2, part, 0.0) for part in erase_pairs]
+        block = 2
+        while block < tokens:
+            keep = (row // (2 * block) == col // (2 * block)) & (row // block != col // block)
+            halves = [
+                dot_nn(inverse[h], jnp.where(keep, erase_pairs[h], 0.0)) for h in range(2)
+            ]
+            inverse = [inverse[h] + dot_nn(halves[h], inverse[h]) for h in range(2)]
+            block *= 2
+        rhs = [jnp.concatenate([dot_nn(part, val), before], axis=1) for part in write_pairs]
+        solved = [dot_nn(inverse[h], rhs[h]) for h in range(2)]
         for h in range(2):
-            left = jnp.concatenate([before * lane_masks[h], read * lane_masks[h]], axis=0)
-            prods = dot_nt(left, right)
-            erase_pairs = jnp.where(strict, prods[:tokens, :tokens], 0.0)
-            write_pairs = jnp.where(strict, prods[:tokens, tokens:], 0.0)
-            pairs_re.append(jnp.where(inclusive, prods[tokens:, :tokens], 0.0))
-            pairs_rw.append(jnp.where(inclusive, prods[tokens:, tokens:], 0.0))
-            inverse = eye_tok + jnp.where(row // 2 == col // 2, erase_pairs, 0.0)
-            block = 2
-            while block < tokens:
-                step = jnp.where(
-                    (row // (2 * block) == col // (2 * block)) & (row // block != col // block),
-                    erase_pairs,
-                    0.0,
-                )
-                inverse = inverse + dot_nn(dot_nn(inverse, step), inverse)
-                block *= 2
-            rhs = jnp.concatenate([dot_nn(write_pairs, val), before], axis=1)
-            solved = dot_nn(inverse, rhs)
-            removed = removed + lane_masks[h] * solved[:, :pair]
-            carried = carried + lane_masks[h] * solved[:, pair:]
+            removed = removed + lane_masks[h] * solved[h][:, :pair]
+            carried = carried + lane_masks[h] * solved[h][:, pair:]
         local_out = jnp.zeros((tokens, pair), f32)
         query = read
         both = jnp.concatenate([removed, carried], axis=1)

time: 110 us -> 103 us (0.936)
  Pallas kernels: 107 us -> 100 us
    pallas_call x1, Pallas kernels: 69 us -> 62.5 us  [expert_layer(): pl.pallas_call(functools.partial(expert_kernel, n_sp, n_tp, cap), out_sha...]
where the time goes in v4:
time: 103 us
  Pallas kernels  100 us (97%)
  local copies, waits for them, and re-layouts  1.57 us (2%)
  other arithmetic  1.41 us (1%)
    pallas_call x1, Pallas kernels, expert_layer(): pl.pallas_call(functools.partial(expert_kernel, n_sp, n_tp, cap), out_sha...  62.5 us
    pallas_call x1, Pallas kernels, memory_and_norm(): pl.pallas_call(functools.partial(memory_kernel, n_sp, n_tp), out_shape=[j...  37.7 us

profile of v4, /device:TPU:0, one launch (start us, length us, event | category | flops | bytes accessed | tf_op | source)
XLA Modules:
  0.0 103.1 jit_solution(14729346235255458687)
XLA Ops:
  0.0 37.7 %memory_and_norm.1 = (bf16[128,2048]{1,0:T(8,128)(2,1)}, bf16[128,2048]{1,0:T(8,128)(2,1)}, bf16[128,512]{1,0:T(8,128)(2,1)}) custom-call(bf16[128,256]{1,0:T(8,128)(2,1)} %r_ref.1, bf16[128,256]{1,0:T(8,128)(2,1)} %k_ref.1, bf16[128,256]{1,0:T(8,128)(2,1)} %v_ref.1, bf16[128,256]{1,0:T(8,128)(2,1)} %d_ref.1, bf16[128,256]{1,0:T(8,128)(2,1)} %c_ref.1, ...), custom_call_target="tpu_custom_call" | custom-call | tf_op jit(solution)/shard_map/memory_and_norm/pallas_call | solution.py:319
  37.7 1.4 %fusion.wt_ref = f32[8,8,128]{2,1,0:T(8,128)} fusion(f32[8,128]{1,0:T(8,128)} %bitcast.12, s32[8,128]{1,0:T(8,128)} %bitcast.13, s32[8]{0:T(128)S(1)} %multiply_add_fusion), kind=kOutput, calls=%fused_computation | output fusion | flops 17415 | bytes 40992 | tf_op jit(solution)/shard_map/broadcast_in_dim | solution.py:818
  39.1 62.5 %expert_layer.1 = bf16[128,512]{1,0:T(8,128)(2,1)} custom-call(bf16[128,2048]{1,0:T(8,128)(2,1)} %get-tuple-element.7.nrm_ref, bf16[128,512]{1,0:T(8,128)(2,1)} %get-tuple-element.8.own_ref, f32[8,8,128]{2,1,0:T(8,128)} %fusion.wt_ref, bf16[1,2048,512]{2,1,0:T(8,128)(2,1)} %gate_hbm.1, bf16[1,2048,512]{2,1,0:T(8,128)(2,1)} %up_hbm.1, ...), custom_call_target="tpu_custom_call" | custom-call | tf_op jit(solution)/shard_map/expert_layer/pallas_call | solution.py:735
  101.6 1.6 %copy.23 = bf16[128,512]{1,0:T(8,128)(2,1)} copy(bf16[128,512]{1,0:T(8,128)(2,1)} %expert_layer.1) | data formatting | bytes 262144
  (1 shorter events, 0.0 us)
